TPU v7x, 32 devices: a whole 2x2x4 slice. The times are simulated.
32 devices in a mesh: sp: 16 (over z, y, x), tp: 2 (over core).
Axes of the slice: x: 2, y: 2, z: 4, core: 2. Of those that a mesh axis runs over, the one named last changes fastest.
Arguments:
- skip_pathway: bfloat16 [2048, 2048], P('sp', 'tp'), may hold values from -6 to 6
- request_vectors: bfloat16 [2048, 1024], P('sp', 'tp'), may hold values from -6 to 6
- lookup_address_matrix: bfloat16 [2048, 1024], P('sp', 'tp'), may hold values from -6 to 6
- content_vectors: bfloat16 [2048, 1024], P('sp', 'tp'), may hold values from -6 to 6
- result_valve_matrix: bfloat16 [2048, 1024], P('sp', 'tp'), may hold values from -6 to 6
- shrink_raw_signal: float32 [2, 8, 2048], P(None, 'tp', 'sp'), may hold values from -3.1 to 3.6
- channel_shrink_speed: float32 [2, 8], P(None, 'tp'), may hold values from 2.4414063e-05 to 0.05
- insertion_raw_signal: float32 [2, 8, 2048], P(None, 'tp', 'sp'), may hold values from -8.5 to 2
- extra_shrink_spike: float32 [2, 8, 2048], P(None, 'tp', 'sp'), may hold values from -1.2 to 0
- channel_scaling_vector: float32 [128], replicated, may hold values from 0.1 to 1.9
- final_mapping_matrix: bfloat16 [1024, 2048], P(None, 'tp'), may hold values from -0.1875 to 0.1875
- mixer_scaling_vector: float32 [2048], replicated, may hold values from 0.1 to 1.9
- valve_matrix: bfloat16 [2048, 5120], P('sp', 'tp'), may hold values from -0.125 to 0.125
- widening_matrix: bfloat16 [2048, 5120], P('sp', 'tp'), may hold values from -0.125 to 0.125
- temporal_kernel_entries: float32 [3, 5120], P(None, 'tp'), may hold values from -3 to 3
- narrowing_matrix: bfloat16 [5120, 2048], P('tp', 'sp'), may hold values from -0.078125 to 0.078125
Outputs:
- result: bfloat16 [2048, 2048], P('sp', 'tp')
All inputs are finite; a program needn't handle non-finite values.
Results may differ from a plain program's by a relative error of at most 0.009.
Values may be sent and summed in bfloat16 or wider, within the bound.
No kernel may reach another device: no remote copies, remote signals or barrier semaphores. Data moves between devices by JAX's collectives and lax.ppermute only.
A program may use at most 128 MiB of HBM per device.

v0:
```python
import jax
import jax.numpy as jnp
from jax import lax
from jax.sharding import PartitionSpec as P

DK = 128
DV = 128
BLOCK = 64


HIGHEST = lax.Precision.HIGHEST


def from_behind(block, axis, distance):
    devices = range(lax.axis_size(axis))
    route = [(i - distance, i) for i in devices if i - distance in devices]
    return lax.ppermute(block, axis, route)


def padded_2(array, sides, width):
    for axis, dim in sides:
        size, length = (lax.axis_size(axis), array.shape[dim])
        up = [(i, (i + 1) % size) for i in range(size - 1)]
        down = [(j, i) for i, j in up]
        last = lax.slice_in_dim(array, length - width, length, axis=dim)
        initial = lax.slice_in_dim(array, 0, width, axis=dim)
        before = lax.ppermute(last, axis, up)
        after = lax.ppermute(initial, axis, down)
        array = jnp.concatenate([before, array, after], axis=dim)
    return array


def heads_of(matrix, head_size):
    return jnp.transpose(
        matrix.astype(jnp.float32).reshape(matrix.shape[0], -1, head_size), (1, 0, 2)
    )


def unit_rows(vectors):
    return vectors * lax.rsqrt(jnp.sum(vectors * vectors, axis=-1, keepdims=True) + 1e-06)


def inverse_unit_lower(strict):
    width = strict.shape[-1]
    identity = jnp.eye(width, dtype=jnp.float32)
    powered = -strict
    result = identity + powered
    covered = 2
    while covered < width:
        powered = jnp.matmul(powered, powered, precision=HIGHEST)
        result = jnp.matmul(result, identity + powered, precision=HIGHEST)
        covered = covered * 2
    return result


def block_parts(queries, keys, values, shrink_exponent, beta, width):
    heads, length, key_size = queries.shape
    value_size = values.shape[-1]
    count = length // width
    queries = queries.reshape(heads, count, width, key_size)
    keys = keys.reshape(heads, count, width, key_size)
    values = values.reshape(heads, count, width, value_size)
    shrink_exponent = shrink_exponent.reshape(heads, count, width)
    beta = beta.reshape(heads, count, width)
    cumulative = jnp.cumsum(shrink_exponent, axis=-1)
    inside = jnp.tril(jnp.ones((width, width), dtype=bool))
    decay = jnp.exp(
        jnp.where(inside, cumulative[..., :, None] - cumulative[..., None, :], -jnp.inf)
    )
    weighted = keys * beta[..., None]
    strict = jnp.tril(jnp.einsum("hnid,hnjd->hnij", weighted, keys, precision=HIGHEST) * decay, -1)
    inverse = inverse_unit_lower(strict)
    writes = jnp.matmul(inverse, values * beta[..., None], precision=HIGHEST)
    erases = jnp.matmul(inverse, weighted * jnp.exp(cumulative)[..., None], precision=HIGHEST)
    within = jnp.einsum("hnid,hnjd->hnij", queries, keys, precision=HIGHEST) * decay
    query_decayed = queries * jnp.exp(cumulative)[..., None]
    keys_decayed = keys * jnp.exp(cumulative[..., -1:] - cumulative)[..., None]
    block_decay = jnp.exp(cumulative[..., -1])
    return (query_decayed, keys_decayed, erases, writes, within, block_decay)


def run_blocks(parts, state):

    def advance(carry, block):
        query_decayed, keys_decayed, erases, writes, within, block_decay = block
        fresh = writes - jnp.matmul(erases, carry, precision=HIGHEST)
        output = jnp.matmul(query_decayed, carry, precision=HIGHEST) + jnp.matmul(
            within, fresh, precision=HIGHEST
        )
        carry = carry * block_decay[:, None, None] + jnp.matmul(
            jnp.swapaxes(keys_decayed, -1, -2), fresh, precision=HIGHEST
        )
        return (carry, output)

    blocks = tuple((jnp.moveaxis(item, 1, 0) for item in parts))
    final, outputs = lax.scan(advance, state, blocks)
    outputs = jnp.moveaxis(outputs, 0, 1)
    return outputs.reshape(outputs.shape[0], -1, outputs.shape[-1])


def compose_map(parts):
    query_decayed, keys_decayed, erases, writes, within, block_decay = parts
    heads, count, width, key_size = keys_decayed.shape
    identity = jnp.eye(key_size, dtype=jnp.float32)
    turned = jnp.swapaxes(keys_decayed, -1, -2)
    transitions = block_decay[..., None, None] * identity - jnp.matmul(
        turned, erases, precision=HIGHEST
    )
    additions = jnp.matmul(turned, writes, precision=HIGHEST)

    def absorb(carry, block):
        matrix, state = carry
        transition, addition = block
        matrix = jnp.matmul(transition, matrix, precision=HIGHEST)
        state = jnp.matmul(transition, state, precision=HIGHEST) + addition
        return ((matrix, state), None)

    start = (
        jnp.broadcast_to(identity, (heads, key_size, key_size)),
        jnp.zeros((heads, key_size, writes.shape[-1]), jnp.float32),
    )
    result, unused = lax.scan(
        absorb, start, (jnp.moveaxis(transitions, 1, 0), jnp.moveaxis(additions, 1, 0))
    )
    return result


def apply_map(affine, state):
    return jnp.matmul(affine[0], state, precision=HIGHEST) + affine[1]


def gate_heads(mixture, result_valve_matrix, channel_scaling_vector):
    scaled = (
        mixture
        * lax.rsqrt(jnp.mean(mixture * mixture, axis=-1, keepdims=True) + 1e-06)
        * channel_scaling_vector
    )
    gated = scaled * jax.nn.silu(heads_of(result_valve_matrix, mixture.shape[-1]))
    return jnp.transpose(gated, (1, 0, 2)).reshape(gated.shape[1], -1).astype(jnp.bfloat16)


def rms_rows(rows, gain):
    widened = rows.astype(jnp.float32)
    return (
        widened * lax.rsqrt(jnp.mean(widened * widened, axis=-1, keepdims=True) + 1e-06) * gain
    ).astype(jnp.bfloat16)


def body(
    skip_pathway,
    request_vectors,
    lookup_address_matrix,
    content_vectors,
    result_valve_matrix,
    shrink_raw_signal,
    channel_shrink_speed,
    insertion_raw_signal,
    extra_shrink_spike,
    channel_scaling_vector,
    final_mapping_matrix,
    mixer_scaling_vector,
    valve_matrix,
    widening_matrix,
    temporal_kernel_entries,
    narrowing_matrix,
):
    queries = unit_rows(heads_of(request_vectors, DK)) * DK ** (-0.5)
    keys = unit_rows(heads_of(lookup_address_matrix, DK))
    values = heads_of(content_vectors, DV)
    shrink_exponent = (
        -channel_shrink_speed[:, :, None] * jax.nn.softplus(shrink_raw_signal) + extra_shrink_spike
    )
    beta = jax.nn.sigmoid(insertion_raw_signal)
    ahead = block_parts(queries, keys, values, shrink_exponent[0], beta[0], BLOCK)
    behind = block_parts(
        jnp.flip(queries, 1),
        jnp.flip(keys, 1),
        jnp.flip(values, 1),
        jnp.flip(shrink_exponent[1], 1),
        jnp.flip(beta[1], 1),
        BLOCK,
    )
    map_ahead = compose_map(ahead)
    map_behind = compose_map(behind)
    heads = queries.shape[0]

    def relay(turn, states):
        state_ahead = from_behind(apply_map(map_ahead, states[0]), "sp", 1)
        state_behind = from_behind(apply_map(map_behind, states[1]), "sp", -1)
        return (state_ahead, state_behind)

    empty = jnp.zeros((heads, DK, DV), jnp.float32)
    start_ahead, start_behind = lax.fori_loop(0, lax.axis_size("sp") - 1, relay, (empty, empty))
    forward = run_blocks(ahead, start_ahead)
    backward = jnp.flip(run_blocks(behind, start_behind), 1)
    mixed = gate_heads(forward + backward, result_valve_matrix, channel_scaling_vector)
    projected = jnp.dot(
        lax.all_gather(mixed, "tp", axis=1, tiled=True),
        final_mapping_matrix,
        preferred_element_type=jnp.float32,
    )
    middle = (skip_pathway.astype(jnp.float32) + projected).astype(jnp.bfloat16)
    full_rows = lax.all_gather(middle, "tp", axis=1, tiled=True)
    normed = rms_rows(full_rows, mixer_scaling_vector)

    def add_features(piece):
        return jnp.dot(normed, piece, preferred_element_type=jnp.float32)

    gate = add_features(lax.all_gather(valve_matrix, "sp", axis=0, tiled=True))
    up = add_features(lax.all_gather(widening_matrix, "sp", axis=0, tiled=True))
    gate = gate.astype(jnp.bfloat16)
    padded = padded_2(gate, (("sp", 0),), 1).astype(jnp.float32)
    convolved = (
        padded[:-2] * temporal_kernel_entries[0]
        + padded[1:-1] * temporal_kernel_entries[1]
        + padded[2:] * temporal_kernel_entries[2]
    )
    hidden = (jax.nn.silu(convolved) * up).astype(jnp.bfloat16)
    terms = jnp.dot(
        hidden,
        lax.all_gather(narrowing_matrix, "sp", axis=1, tiled=True),
        preferred_element_type=jnp.float32,
    )
    summed = lax.psum_scatter(
        terms.astype(jnp.bfloat16), "tp", scatter_dimension=1, tiled=True
    ).astype(jnp.float32)
    return (middle.astype(jnp.float32) + summed).astype(jnp.bfloat16)


def solution(mesh):
    return jax.shard_map(
        body,
        mesh=mesh,
        in_specs=(
            P("sp", "tp"),
            P("sp", "tp"),
            P("sp", "tp"),
            P("sp", "tp"),
            P("sp", "tp"),
            P(None, "tp", "sp"),
            P(None, "tp"),
            P(None, "tp", "sp"),
            P(None, "tp", "sp"),
            P(),
            P(None, "tp"),
            P(),
            P("sp", "tp"),
            P("sp", "tp"),
            P(None, "tp"),
            P("tp", "sp"),
        ),
        out_specs=P("sp", "tp"),
        check_vma=False,
    )
```

profile of v0, /device:TPU:0, one launch (start us, length us, event | category | flops | bytes accessed | tf_op | source)
XLA Modules:
  0.0 573.6 jit_solution(4285301047786640406)
XLA Ops:
  66.7 352.4 %while.62 = (s32[]{:T(128)}, f32[4,128,128]{2,1,0:T(8,128)S(1)}, f32[4,128,128]{2,1,0:T(8,128)S(1)}, f32[4,128,128]{2,1,0:T(8,128)S(1)}, f32[4,128,128]{2,1,0:T(...) while((s32[]{:T(128)}, f32[4,128,128]{2,1,0:T(8,128)S(1)}, ...), condition=%wide.region_8.9_spmd, body=%wide.region_7.8_spmd.sunk | while | flops 201457664 | bytes 4194469 | solution.py:193
  68.7 5.0 collective-permute-start
  79.6 11.4 %collective-permute-done.1 = f32[4,128,128]{2,1,0:T(8,128)S(1)} collective-permute-done((f32[4,128,128]{2,1,0:T(8,128)}, f32[4,128,128]{2,1,0:T(8,128)S(1)}, u32[]{:S(2)}, u32[]{:S(2)}) %collective-permute-start.1) | collective-permute-done | bytes 262176 | tf_op jit(solution)/shard_map/while/body/eval_jaxpr/ppermute | solution.py:17
  98.8 10.1 %collective-permute-done = f32[4,128,128]{2,1,0:T(8,128)S(1)} collective-permute-done((f32[4,128,128]{2,1,0:T(8,128)}, f32[4,128,128]{2,1,0:T(8,128)S(1)}, u32[]{:S(2)}, u32[]{:S(2)}) %collective-permute-start) | collective-permute-done | bytes 262176 | tf_op jit(solution)/shard_map/while/body/eval_jaxpr/ppermute | solution.py:17
  109.0 10.5 %collective-permute-done.1 = f32[4,128,128]{2,1,0:T(8,128)S(1)} collective-permute-done((f32[4,128,128]{2,1,0:T(8,128)}, f32[4,128,128]{2,1,0:T(8,128)S(1)}, u32[]{:S(2)}, u32[]{:S(2)}) %collective-permute-start.1) | collective-permute-done | bytes 262176 | tf_op jit(solution)/shard_map/while/body/eval_jaxpr/ppermute | solution.py:17
  121.5 6.4 %collective-permute-start = (f32[4,128,128]{2,1,0:T(8,128)}, f32[4,128,128]{2,1,0:T(8,128)S(1)}, u32[]{:S(2)}, u32[]{:S(2)}) collective-permute-start(f32[4,128,128]{2,1,0:T(8,128)} %convolution_add_fusion.17), channel_id=1, source_target_pairs={{0,2},{2,4},{4,6},{6,8},{8,10},{10,12},{12,14},{14,16},{16,18},{18... | collective-permute-start | bytes 786440 | tf_op jit(solution)/shard_map/while/body/eval_jaxpr/ppermute | solution.py:17
  130.2 13.2 %collective-permute-done = f32[4,128,128]{2,1,0:T(8,128)S(1)} collective-permute-done((f32[4,128,128]{2,1,0:T(8,128)}, f32[4,128,128]{2,1,0:T(8,128)S(1)}, u32[]{:S(2)}, u32[]{:S(2)}) %collective-permute-start) | collective-permute-done | bytes 262176 | tf_op jit(solution)/shard_map/while/body/eval_jaxpr/ppermute | solution.py:17
  156.8 6.3 %collective-permute-done.1 = f32[4,128,128]{2,1,0:T(8,128)S(1)} collective-permute-done((f32[4,128,128]{2,1,0:T(8,128)}, f32[4,128,128]{2,1,0:T(8,128)S(1)}, u32[]{:S(2)}, u32[]{:S(2)}) %collective-permute-start.1) | collective-permute-done | bytes 262176 | tf_op jit(solution)/shard_map/while/body/eval_jaxpr/ppermute | solution.py:17
  169.4 5.0 collective-permute-done
  180.5 19.1 %collective-permute-start = (f32[4,128,128]{2,1,0:T(8,128)}, f32[4,128,128]{2,1,0:T(8,128)S(1)}, u32[]{:S(2)}, u32[]{:S(2)}) collective-permute-start(f32[4,128,128]{2,1,0:T(8,128)} %convolution_add_fusion.17), channel_id=1, source_target_pairs={{0,2},{2,4},{4,6},{6,8},{8,10},{10,12},{12,14},{14,16},{16,18},{18... | collective-permute-start | bytes 786440 | tf_op jit(solution)/shard_map/while/body/eval_jaxpr/ppermute | solution.py:17
  203.8 5.9 %collective-permute-done.1 = f32[4,128,128]{2,1,0:T(8,128)S(1)} collective-permute-done((f32[4,128,128]{2,1,0:T(8,128)}, f32[4,128,128]{2,1,0:T(8,128)S(1)}, u32[]{:S(2)}, u32[]{:S(2)}) %collective-permute-start.1) | collective-permute-done | bytes 262176 | tf_op jit(solution)/shard_map/while/body/eval_jaxpr/ppermute | solution.py:17
  217.2 9.4 %collective-permute-done = f32[4,128,128]{2,1,0:T(8,128)S(1)} collective-permute-done((f32[4,128,128]{2,1,0:T(8,128)}, f32[4,128,128]{2,1,0:T(8,128)S(1)}, u32[]{:S(2)}, u32[]{:S(2)}) %collective-permute-start) | collective-permute-done | bytes 262176 | tf_op jit(solution)/shard_map/while/body/eval_jaxpr/ppermute | solution.py:17
  226.6 11.2 %collective-permute-done.1 = f32[4,128,128]{2,1,0:T(8,128)S(1)} collective-permute-done((f32[4,128,128]{2,1,0:T(8,128)}, f32[4,128,128]{2,1,0:T(8,128)S(1)}, u32[]{:S(2)}, u32[]{:S(2)}) %collective-permute-start.1) | collective-permute-done | bytes 262176 | tf_op jit(solution)/shard_map/while/body/eval_jaxpr/ppermute | solution.py:17
  239.9 6.8 %collective-permute-start = (f32[4,128,128]{2,1,0:T(8,128)}, f32[4,128,128]{2,1,0:T(8,128)S(1)}, u32[]{:S(2)}, u32[]{:S(2)}) collective-permute-start(f32[4,128,128]{2,1,0:T(8,128)} %convolution_add_fusion.17), channel_id=1, source_target_pairs={{0,2},{2,4},{4,6},{6,8},{8,10},{10,12},{12,14},{14,16},{16,18},{18... | collective-permute-start | bytes 786440 | tf_op jit(solution)/shard_map/while/body/eval_jaxpr/ppermute | solution.py:17
  251.0 5.9 %collective-permute-done.1 = f32[4,128,128]{2,1,0:T(8,128)S(1)} collective-permute-done((f32[4,128,128]{2,1,0:T(8,128)}, f32[4,128,128]{2,1,0:T(8,128)S(1)}, u32[]{:S(2)}, u32[]{:S(2)}) %collective-permute-start.1) | collective-permute-done | bytes 262176 | tf_op jit(solution)/shard_map/while/body/eval_jaxpr/ppermute | solution.py:17
  266.2 16.1 %collective-permute-done.1 = f32[4,128,128]{2,1,0:T(8,128)S(1)} collective-permute-done((f32[4,128,128]{2,1,0:T(8,128)}, f32[4,128,128]{2,1,0:T(8,128)S(1)}, u32[]{:S(2)}, u32[]{:S(2)}) %collective-permute-start.1) | collective-permute-done | bytes 262176 | tf_op jit(solution)/shard_map/while/body/eval_jaxpr/ppermute | solution.py:17
  284.4 7.8 %collective-permute-start = (f32[4,128,128]{2,1,0:T(8,128)}, f32[4,128,128]{2,1,0:T(8,128)S(1)}, u32[]{:S(2)}, u32[]{:S(2)}) collective-permute-start(f32[4,128,128]{2,1,0:T(8,128)} %convolution_add_fusion.17), channel_id=1, source_target_pairs={{0,2},{2,4},{4,6},{6,8},{8,10},{10,12},{12,14},{14,16},{16,18},{18... | collective-permute-start | bytes 786440 | tf_op jit(solution)/shard_map/while/body/eval_jaxpr/ppermute | solution.py:17
  294.6 7.5 %collective-permute-done = f32[4,128,128]{2,1,0:T(8,128)S(1)} collective-permute-done((f32[4,128,128]{2,1,0:T(8,128)}, f32[4,128,128]{2,1,0:T(8,128)S(1)}, u32[]{:S(2)}, u32[]{:S(2)}) %collective-permute-start) | collective-permute-done | bytes 262176 | tf_op jit(solution)/shard_map/while/body/eval_jaxpr/ppermute | solution.py:17
  302.1 11.1 %collective-permute-done.1 = f32[4,128,128]{2,1,0:T(8,128)S(1)} collective-permute-done((f32[4,128,128]{2,1,0:T(8,128)}, f32[4,128,128]{2,1,0:T(8,128)S(1)}, u32[]{:S(2)}, u32[]{:S(2)}) %collective-permute-start.1) | collective-permute-done | bytes 262176 | tf_op jit(solution)/shard_map/while/body/eval_jaxpr/ppermute | solution.py:17
  315.2 9.2 %collective-permute-start = (f32[4,128,128]{2,1,0:T(8,128)}, f32[4,128,128]{2,1,0:T(8,128)S(1)}, u32[]{:S(2)}, u32[]{:S(2)}) collective-permute-start(f32[4,128,128]{2,1,0:T(8,128)} %convolution_add_fusion.17), channel_id=1, source_target_pairs={{0,2},{2,4},{4,6},{6,8},{8,10},{10,12},{12,14},{14,16},{16,18},{18... | collective-permute-start | bytes 786440 | tf_op jit(solution)/shard_map/while/body/eval_jaxpr/ppermute | solution.py:17
  328.6 5.4 collective-permute-done.1
  347.3 5.3 collective-permute-done.1
  354.7 17.2 %collective-permute-start = (f32[4,128,128]{2,1,0:T(8,128)}, f32[4,128,128]{2,1,0:T(8,128)S(1)}, u32[]{:S(2)}, u32[]{:S(2)}) collective-permute-start(f32[4,128,128]{2,1,0:T(8,128)} %convolution_add_fusion.17), channel_id=1, source_target_pairs={{0,2},{2,4},{4,6},{6,8},{8,10},{10,12},{12,14},{14,16},{16,18},{18... | collective-permute-start | bytes 786440 | tf_op jit(solution)/shard_map/while/body/eval_jaxpr/ppermute | solution.py:17
  374.3 12.6 %collective-permute-done = f32[4,128,128]{2,1,0:T(8,128)S(1)} collective-permute-done((f32[4,128,128]{2,1,0:T(8,128)}, f32[4,128,128]{2,1,0:T(8,128)S(1)}, u32[]{:S(2)}, u32[]{:S(2)}) %collective-permute-start) | collective-permute-done | bytes 262176 | tf_op jit(solution)/shard_map/while/body/eval_jaxpr/ppermute | solution.py:17
  399.6 4.8 collective-permute-done.1
  419.8 10.3 %while.64 = (s32[]{:T(128)}, f32[4,128,128]{2,1,0:T(8,128)S(1)}, f32[2,4,64,128]{3,2,0,1:T(8,128)}, f32[2,4]{1,0:T(2,128)S(1)}, f32[2,4,64,128]{3,2,0,1:T(8,128)...) while((s32[]{:T(128)}, f32[4,128,128]{2,1,0:T(8,128)S(1)}, ...), condition=%wide.region_13.14_spmd, body=%wide.region_12.13_spmd.sunk | while | flops 176357376 | bytes 3542185 | solution.py:96
  439.2 6.5 %while.63 = (s32[]{:T(128)}, f32[4,128,128]{2,1,0:T(8,128)S(1)}, f32[2,4,64,128]{3,2,0,1:T(8,128)}, f32[2,4]{1,0:T(2,128)S(1)}, f32[2,4,64,128]{3,2,0,1:T(8,128)...) while((s32[]{:T(128)}, f32[4,128,128]{2,1,0:T(8,128)S(1)}, ...), condition=%wide.region_11.12_spmd, body=%wide.region_10.11_spmd.sunk | while | flops 176357376 | bytes 3541677 | solution.py:96
  453.2 5.7 %convolution_convert_fusion = bf16[128,2560]{1,0:T(8,128)(2,1)S(1)} fusion(bf16[2048,2560]{1,0:T(8,128)(2,1)} %all-gather.4.cloned.1.call-done, bf16[128,2048]{1,0:T(8,128)(2,1)S(1)} %all_gather.16, f32[2048]{0:T(1024)S(1)} %copy-done.20, f32[128]{0:T(128)S(1)} %add_rsqrt_fusion.3), kind=kOutput, calls=%fused_computation.68 | convolution fusion | flops 1343553536 | bytes 11674112 | tf_op jit(solution)/shard_map/dot_general | solution.py:207
  459.0 9.3 %collective-permute-start.2 = (bf16[1,2560]{1,0:T(2,128)(2,1)S(1)}, bf16[1,2560]{1,0:T(2,128)(2,1)S(1)}, u32[]{:S(2)}, u32[]{:S(2)}) collective-permute-start(bf16[1,2560]{1,0:T(2,128)(2,1)S(1)} %get-tuple-element.394), channel_id=1, source_target_pairs={{0,2},{2,4},{4,6},{6,8},{8,10},{10,12},{12,14},{14,16},{16,18},{18... | collective-permute-start | bytes 15368 | tf_op jit(solution)/shard_map/ppermute | solution.py:27
  475.6 70.7 %all-gather.8.cloned.1.call-done = bf16[2560,2048]{1,0:T(8,128)(2,1)} async-done(((bf16[2560,128]{1,0:T(8,128)(2,1)}), bf16[2560,2048]{1,0:T(8,128)(2,1)}) %all-gather.8.cloned.1.call-update) | async-done | bytes 10485776 | tf_op jit(solution)/shard_map/all_gather | solution.py:221
  546.3 12.8 %convolution_convert_fusion.1 = bf16[128,2048]{1,0:T(8,128)(2,1)} fusion(bf16[2560,2048]{1,0:T(8,128)(2,1)} %all-gather.8.cloned.1.call-done, bf16[2048,2560]{1,0:T(8,128)(2,1)} %all-gather.6.cloned.1.call-done, f32[130,2560]{1,0:T(8,128)} %maximum_convert_fusion, f32[2560]{0:T(1024)S(1)} %get-tuple-element.322, f32[2560]{0:T(1024)S(1)} %get-tuple-element.323, ...), kind=kOutput, calls=%fused_computation.69 | convolution fusion | flops 2689269760 | bytes 25991680 | tf_op jit(solution)/shard_map/dot_general | solution.py:219
  559.1 6.2 %reduce-scatter.2.cloned.1.call-done = bf16[128,1024]{1,0:T(8,128)(2,1)} async-done(((bf16[128,2048]{1,0:T(8,128)(2,1)}), bf16[128,1024]{1,0:T(8,128)(2,1)}) %reduce-scatter.2.cloned.1.call-update) | async-done | bytes 262160 | tf_op jit(solution)/shard_map/reduce_scatter | solution.py:224
  (284 shorter events, 238.7 us)
Async XLA Ops:
  6.5 446.7 %all-gather.4.cloned.1.call-start = ((), (), s32[]{:S(2)}) async-start(), calls=%async_computation.1 | async-start | bytes 11141120 | tf_op jit(solution)/shard_map/all_gather | solution.py:209
  7.3 468.3 %all-gather.6.cloned.1.call-start = ((), (), s32[]{:S(2)}) async-start(), calls=%async_computation.2 | async-start | bytes 11141120 | tf_op jit(solution)/shard_map/all_gather | solution.py:210
  8.0 538.3 %all-gather.8.cloned.1.call-start = ((), (), s32[]{:S(2)}) async-start(), calls=%async_computation.3 | async-start | bytes 11141120 | tf_op jit(solution)/shard_map/all_gather | solution.py:221
  8.8 556.6 %reduce-scatter.2.cloned.1.call-start = ((), (), s32[]{:S(2)}) async-start(), calls=%async_computation.4 | async-start | bytes 786432 | tf_op jit(solution)/shard_map/reduce_scatter | solution.py:224
  68.7 10.8 %collective-permute-start = (f32[4,128,128]{2,1,0:T(8,128)}, f32[4,128,128]{2,1,0:T(8,128)S(1)}, u32[]{:S(2)}, u32[]{:S(2)}) collective-permute-start(f32[4,128,128]{2,1,0:T(8,128)} %convolution_add_fusion.17), channel_id=1, source_target_pairs={{0,2},{2,4},{4,6},{6,8},{8,10},{10,12},{12,14},{14,16},{16,18},{18... | collective-permute-start | bytes 786440 | tf_op jit(solution)/shard_map/while/body/eval_jaxpr/ppermute | solution.py:17
  74.8 16.2 %collective-permute-start.1 = (f32[4,128,128]{2,1,0:T(8,128)}, f32[4,128,128]{2,1,0:T(8,128)S(1)}, u32[]{:S(2)}, u32[]{:S(2)}) collective-permute-start(f32[4,128,128]{2,1,0:T(8,128)} %convolution_add_fusion.18), channel_id=1, source_target_pairs={{2,0},{4,2},{6,4},{8,6},{10,8},{12,10},{14,12},{16,14},{18,16},{20... | collective-permute-start | bytes 786440 | tf_op jit(solution)/shard_map/while/body/eval_jaxpr/ppermute | solution.py:17
  93.0 15.9 %collective-permute-start = (f32[4,128,128]{2,1,0:T(8,128)}, f32[4,128,128]{2,1,0:T(8,128)S(1)}, u32[]{:S(2)}, u32[]{:S(2)}) collective-permute-start(f32[4,128,128]{2,1,0:T(8,128)} %convolution_add_fusion.17), channel_id=1, source_target_pairs={{0,2},{2,4},{4,6},{6,8},{8,10},{10,12},{12,14},{14,16},{16,18},{18... | collective-permute-start | bytes 786440 | tf_op jit(solution)/shard_map/while/body/eval_jaxpr/ppermute | solution.py:17
  97.5 21.9 %collective-permute-start.1 = (f32[4,128,128]{2,1,0:T(8,128)}, f32[4,128,128]{2,1,0:T(8,128)S(1)}, u32[]{:S(2)}, u32[]{:S(2)}) collective-permute-start(f32[4,128,128]{2,1,0:T(8,128)} %convolution_add_fusion.18), channel_id=1, source_target_pairs={{2,0},{4,2},{6,4},{8,6},{10,8},{12,10},{14,12},{16,14},{18,16},{20... | collective-permute-start | bytes 786440 | tf_op jit(solution)/shard_map/while/body/eval_jaxpr/ppermute | solution.py:17
  121.5 21.9 %collective-permute-start = (f32[4,128,128]{2,1,0:T(8,128)}, f32[4,128,128]{2,1,0:T(8,128)S(1)}, u32[]{:S(2)}, u32[]{:S(2)}) collective-permute-start(f32[4,128,128]{2,1,0:T(8,128)} %convolution_add_fusion.17), channel_id=1, source_target_pairs={{0,2},{2,4},{4,6},{6,8},{8,10},{10,12},{12,14},{14,16},{16,18},{18... | collective-permute-start | bytes 786440 | tf_op jit(solution)/shard_map/while/body/eval_jaxpr/ppermute | solution.py:17
  128.9 18.0 %collective-permute-start.1 = (f32[4,128,128]{2,1,0:T(8,128)}, f32[4,128,128]{2,1,0:T(8,128)S(1)}, u32[]{:S(2)}, u32[]{:S(2)}) collective-permute-start(f32[4,128,128]{2,1,0:T(8,128)} %convolution_add_fusion.18), channel_id=1, source_target_pairs={{2,0},{4,2},{6,4},{8,6},{10,8},{12,10},{14,12},{16,14},{18,16},{20... | collective-permute-start | bytes 786440 | tf_op jit(solution)/shard_map/while/body/eval_jaxpr/ppermute | solution.py:17
  153.4 9.6 %collective-permute-start.1 = (f32[4,128,128]{2,1,0:T(8,128)}, f32[4,128,128]{2,1,0:T(8,128)S(1)}, u32[]{:S(2)}, u32[]{:S(2)}) collective-permute-start(f32[4,128,128]{2,1,0:T(8,128)} %convolution_add_fusion.18), channel_id=1, source_target_pairs={{2,0},{4,2},{6,4},{8,6},{10,8},{12,10},{14,12},{16,14},{18,16},{20... | collective-permute-start | bytes 786440 | tf_op jit(solution)/shard_map/while/body/eval_jaxpr/ppermute | solution.py:17
  165.1 9.4 %collective-permute-start = (f32[4,128,128]{2,1,0:T(8,128)}, f32[4,128,128]{2,1,0:T(8,128)S(1)}, u32[]{:S(2)}, u32[]{:S(2)}) collective-permute-start(f32[4,128,128]{2,1,0:T(8,128)} %convolution_add_fusion.17), channel_id=1, source_target_pairs={{0,2},{2,4},{4,6},{6,8},{8,10},{10,12},{12,14},{14,16},{16,18},{18... | collective-permute-start | bytes 786440 | tf_op jit(solution)/shard_map/while/body/eval_jaxpr/ppermute | solution.py:17
  168.1 10.3 %collective-permute-start.1 = (f32[4,128,128]{2,1,0:T(8,128)}, f32[4,128,128]{2,1,0:T(8,128)S(1)}, u32[]{:S(2)}, u32[]{:S(2)}) collective-permute-start(f32[4,128,128]{2,1,0:T(8,128)} %convolution_add_fusion.18), channel_id=1, source_target_pairs={{2,0},{4,2},{6,4},{8,6},{10,8},{12,10},{14,12},{16,14},{18,16},{20... | collective-permute-start | bytes 786440 | tf_op jit(solution)/shard_map/while/body/eval_jaxpr/ppermute | solution.py:17
  180.5 23.3 %collective-permute-start = (f32[4,128,128]{2,1,0:T(8,128)}, f32[4,128,128]{2,1,0:T(8,128)S(1)}, u32[]{:S(2)}, u32[]{:S(2)}) collective-permute-start(f32[4,128,128]{2,1,0:T(8,128)} %convolution_add_fusion.17), channel_id=1, source_target_pairs={{0,2},{2,4},{4,6},{6,8},{8,10},{10,12},{12,14},{14,16},{16,18},{18... | collective-permute-start | bytes 786440 | tf_op jit(solution)/shard_map/while/body/eval_jaxpr/ppermute | solution.py:17
  200.7 9.0 %collective-permute-start.1 = (f32[4,128,128]{2,1,0:T(8,128)}, f32[4,128,128]{2,1,0:T(8,128)S(1)}, u32[]{:S(2)}, u32[]{:S(2)}) collective-permute-start(f32[4,128,128]{2,1,0:T(8,128)} %convolution_add_fusion.18), channel_id=1, source_target_pairs={{2,0},{4,2},{6,4},{8,6},{10,8},{12,10},{14,12},{16,14},{18,16},{20... | collective-permute-start | bytes 786440 | tf_op jit(solution)/shard_map/while/body/eval_jaxpr/ppermute | solution.py:17
  211.8 14.7 %collective-permute-start = (f32[4,128,128]{2,1,0:T(8,128)}, f32[4,128,128]{2,1,0:T(8,128)S(1)}, u32[]{:S(2)}, u32[]{:S(2)}) collective-permute-start(f32[4,128,128]{2,1,0:T(8,128)} %convolution_add_fusion.17), channel_id=1, source_target_pairs={{0,2},{2,4},{4,6},{6,8},{8,10},{10,12},{12,14},{14,16},{16,18},{18... | collective-permute-start | bytes 786440 | tf_op jit(solution)/shard_map/while/body/eval_jaxpr/ppermute | solution.py:17
  215.9 21.9 %collective-permute-start.1 = (f32[4,128,128]{2,1,0:T(8,128)}, f32[4,128,128]{2,1,0:T(8,128)S(1)}, u32[]{:S(2)}, u32[]{:S(2)}) collective-permute-start(f32[4,128,128]{2,1,0:T(8,128)} %convolution_add_fusion.18), channel_id=1, source_target_pairs={{2,0},{4,2},{6,4},{8,6},{10,8},{12,10},{14,12},{16,14},{18,16},{20... | collective-permute-start | bytes 786440 | tf_op jit(solution)/shard_map/while/body/eval_jaxpr/ppermute | solution.py:17
  239.9 11.1 %collective-permute-start = (f32[4,128,128]{2,1,0:T(8,128)}, f32[4,128,128]{2,1,0:T(8,128)S(1)}, u32[]{:S(2)}, u32[]{:S(2)}) collective-permute-start(f32[4,128,128]{2,1,0:T(8,128)} %convolution_add_fusion.17), channel_id=1, source_target_pairs={{0,2},{2,4},{4,6},{6,8},{8,10},{10,12},{12,14},{14,16},{16,18},{18... | collective-permute-start | bytes 786440 | tf_op jit(solution)/shard_map/while/body/eval_jaxpr/ppermute | solution.py:17
  247.8 9.0 %collective-permute-start.1 = (f32[4,128,128]{2,1,0:T(8,128)}, f32[4,128,128]{2,1,0:T(8,128)S(1)}, u32[]{:S(2)}, u32[]{:S(2)}) collective-permute-start(f32[4,128,128]{2,1,0:T(8,128)} %convolution_add_fusion.18), channel_id=1, source_target_pairs={{2,0},{4,2},{6,4},{8,6},{10,8},{12,10},{14,12},{16,14},{18,16},{20... | collective-permute-start | bytes 786440 | tf_op jit(solution)/shard_map/while/body/eval_jaxpr/ppermute | solution.py:17
  262.2 20.1 %collective-permute-start.1 = (f32[4,128,128]{2,1,0:T(8,128)}, f32[4,128,128]{2,1,0:T(8,128)S(1)}, u32[]{:S(2)}, u32[]{:S(2)}) collective-permute-start(f32[4,128,128]{2,1,0:T(8,128)} %convolution_add_fusion.18), channel_id=1, source_target_pairs={{2,0},{4,2},{6,4},{8,6},{10,8},{12,10},{14,12},{16,14},{18,16},{20... | collective-permute-start | bytes 786440 | tf_op jit(solution)/shard_map/while/body/eval_jaxpr/ppermute | solution.py:17
  284.4 17.8 %collective-permute-start = (f32[4,128,128]{2,1,0:T(8,128)}, f32[4,128,128]{2,1,0:T(8,128)S(1)}, u32[]{:S(2)}, u32[]{:S(2)}) collective-permute-start(f32[4,128,128]{2,1,0:T(8,128)} %convolution_add_fusion.17), channel_id=1, source_target_pairs={{0,2},{2,4},{4,6},{6,8},{8,10},{10,12},{12,14},{14,16},{16,18},{18... | collective-permute-start | bytes 786440 | tf_op jit(solution)/shard_map/while/body/eval_jaxpr/ppermute | solution.py:17
  293.3 19.9 %collective-permute-start.1 = (f32[4,128,128]{2,1,0:T(8,128)}, f32[4,128,128]{2,1,0:T(8,128)S(1)}, u32[]{:S(2)}, u32[]{:S(2)}) collective-permute-start(f32[4,128,128]{2,1,0:T(8,128)} %convolution_add_fusion.18), channel_id=1, source_target_pairs={{2,0},{4,2},{6,4},{8,6},{10,8},{12,10},{14,12},{16,14},{18,16},{20... | collective-permute-start | bytes 786440 | tf_op jit(solution)/shard_map/while/body/eval_jaxpr/ppermute | solution.py:17
  315.2 13.4 %collective-permute-start = (f32[4,128,128]{2,1,0:T(8,128)}, f32[4,128,128]{2,1,0:T(8,128)S(1)}, u32[]{:S(2)}, u32[]{:S(2)}) collective-permute-start(f32[4,128,128]{2,1,0:T(8,128)} %convolution_add_fusion.17), channel_id=1, source_target_pairs={{0,2},{2,4},{4,6},{6,8},{8,10},{10,12},{12,14},{14,16},{16,18},{18... | collective-permute-start | bytes 786440 | tf_op jit(solution)/shard_map/while/body/eval_jaxpr/ppermute | solution.py:17
  325.6 8.5 %collective-permute-start.1 = (f32[4,128,128]{2,1,0:T(8,128)}, f32[4,128,128]{2,1,0:T(8,128)S(1)}, u32[]{:S(2)}, u32[]{:S(2)}) collective-permute-start(f32[4,128,128]{2,1,0:T(8,128)} %convolution_add_fusion.18), channel_id=1, source_target_pairs={{2,0},{4,2},{6,4},{8,6},{10,8},{12,10},{14,12},{16,14},{18,16},{20... | collective-permute-start | bytes 786440 | tf_op jit(solution)/shard_map/while/body/eval_jaxpr/ppermute | solution.py:17
  336.1 11.2 %collective-permute-start = (f32[4,128,128]{2,1,0:T(8,128)}, f32[4,128,128]{2,1,0:T(8,128)S(1)}, u32[]{:S(2)}, u32[]{:S(2)}) collective-permute-start(f32[4,128,128]{2,1,0:T(8,128)} %convolution_add_fusion.17), channel_id=1, source_target_pairs={{0,2},{2,4},{4,6},{6,8},{8,10},{10,12},{12,14},{14,16},{16,18},{18... | collective-permute-start | bytes 786440 | tf_op jit(solution)/shard_map/while/body/eval_jaxpr/ppermute | solution.py:17
  341.4 11.2 %collective-permute-start.1 = (f32[4,128,128]{2,1,0:T(8,128)}, f32[4,128,128]{2,1,0:T(8,128)S(1)}, u32[]{:S(2)}, u32[]{:S(2)}) collective-permute-start(f32[4,128,128]{2,1,0:T(8,128)} %convolution_add_fusion.18), channel_id=1, source_target_pairs={{2,0},{4,2},{6,4},{8,6},{10,8},{12,10},{14,12},{16,14},{18,16},{20... | collective-permute-start | bytes 786440 | tf_op jit(solution)/shard_map/while/body/eval_jaxpr/ppermute | solution.py:17
  354.7 32.3 %collective-permute-start = (f32[4,128,128]{2,1,0:T(8,128)}, f32[4,128,128]{2,1,0:T(8,128)S(1)}, u32[]{:S(2)}, u32[]{:S(2)}) collective-permute-start(f32[4,128,128]{2,1,0:T(8,128)} %convolution_add_fusion.17), channel_id=1, source_target_pairs={{0,2},{2,4},{4,6},{6,8},{8,10},{10,12},{12,14},{14,16},{16,18},{18... | collective-permute-start | bytes 786440 | tf_op jit(solution)/shard_map/while/body/eval_jaxpr/ppermute | solution.py:17
  373.0 15.6 %collective-permute-start.1 = (f32[4,128,128]{2,1,0:T(8,128)}, f32[4,128,128]{2,1,0:T(8,128)S(1)}, u32[]{:S(2)}, u32[]{:S(2)}) collective-permute-start(f32[4,128,128]{2,1,0:T(8,128)} %convolution_add_fusion.18), channel_id=1, source_target_pairs={{2,0},{4,2},{6,4},{8,6},{10,8},{12,10},{14,12},{16,14},{18,16},{20... | collective-permute-start | bytes 786440 | tf_op jit(solution)/shard_map/while/body/eval_jaxpr/ppermute | solution.py:17
  390.6 9.0 %collective-permute-start = (f32[4,128,128]{2,1,0:T(8,128)}, f32[4,128,128]{2,1,0:T(8,128)S(1)}, u32[]{:S(2)}, u32[]{:S(2)}) collective-permute-start(f32[4,128,128]{2,1,0:T(8,128)} %convolution_add_fusion.17), channel_id=1, source_target_pairs={{0,2},{2,4},{4,6},{6,8},{8,10},{10,12},{12,14},{14,16},{16,18},{18... | collective-permute-start | bytes 786440 | tf_op jit(solution)/shard_map/while/body/eval_jaxpr/ppermute | solution.py:17
  394.4 10.0 %collective-permute-start.1 = (f32[4,128,128]{2,1,0:T(8,128)}, f32[4,128,128]{2,1,0:T(8,128)S(1)}, u32[]{:S(2)}, u32[]{:S(2)}) collective-permute-start(f32[4,128,128]{2,1,0:T(8,128)} %convolution_add_fusion.18), channel_id=1, source_target_pairs={{2,0},{4,2},{6,4},{8,6},{10,8},{12,10},{14,12},{16,14},{18,16},{20... | collective-permute-start | bytes 786440 | tf_op jit(solution)/shard_map/while/body/eval_jaxpr/ppermute | solution.py:17
  409.5 9.5 %collective-permute-start.1 = (f32[4,128,128]{2,1,0:T(8,128)}, f32[4,128,128]{2,1,0:T(8,128)S(1)}, u32[]{:S(2)}, u32[]{:S(2)}) collective-permute-start(f32[4,128,128]{2,1,0:T(8,128)} %convolution_add_fusion.18), channel_id=1, source_target_pairs={{2,0},{4,2},{6,4},{8,6},{10,8},{12,10},{14,12},{16,14},{18,16},{20... | collective-permute-start | bytes 786440 | tf_op jit(solution)/shard_map/while/body/eval_jaxpr/ppermute | solution.py:17
  459.0 10.8 %collective-permute-start.2 = (bf16[1,2560]{1,0:T(2,128)(2,1)S(1)}, bf16[1,2560]{1,0:T(2,128)(2,1)S(1)}, u32[]{:S(2)}, u32[]{:S(2)}) collective-permute-start(bf16[1,2560]{1,0:T(2,128)(2,1)S(1)} %get-tuple-element.394), channel_id=1, source_target_pairs={{0,2},{2,4},{4,6},{6,8},{8,10},{10,12},{12,14},{14,16},{16,18},{18... | collective-permute-start | bytes 15368 | tf_op jit(solution)/shard_map/ppermute | solution.py:27
  (34 other events, 681.2 us)
Sparse Core Ops, SparseCore 0:
  10.0 162.4 all-gather.3
  175.2 183.1 all-gather.5
  361.1 185.1 all-gather.7
  559.2 6.0 reduce-scatter.1
where the time goes:
time: 576 us; the launch traced here: 574 us
  waiting for transfers between devices  275 us (48%)
  starting transfers between devices  124 us (22%)
  matrix products  122 us (21%)
  local copies, waits for them, and re-layouts  20.5 us (4%)
  between operations  13.8 us (2%)
  other arithmetic  13.5 us (2%)
    ppermute x30, waiting for transfers between devices, from_behind(): return lax.ppermute(block, axis, route)  191 us
    ppermute x30, starting transfers between devices, from_behind(): return lax.ppermute(block, axis, route)  113 us
    all_gather x1, waiting for transfers between devices, body(): lax.all_gather(narrowing_matrix, 'sp', axis=1, tiled=True)  70.7 us
    dot_general x30, matrix products, apply_map(): return jnp.matmul(affine[0], state, precision=HIGHEST) + affine[1]  47.3 us
    dot_general x1, matrix products, body(): jnp.dot(hidden, lax.all_gather(narrowing_matrix, 'sp', axis=1, tiled=True...  12.8 us
  transfers between devices with their start and end apart: 36, of which 34 were waited for; matrix products, arithmetic and copies ran while one was open for 24% of the time, Pallas kernels for 0%

commit v1 on v0

v1 whole, which is shorter than its diff:
```python
import functools
import jax
import jax.numpy as jnp
from jax import lax
from jax.experimental import pallas as pl
from jax.experimental.pallas import tpu as pltpu
from jax.sharding import Mesh, PartitionSpec as P

DK = 128
EPS = 1e-06
F32 = jnp.float32
BF16 = jnp.bfloat16


def halves(x):
    high = x.astype(BF16)
    return high, (x - high.astype(F32)).astype(BF16)


def contract(a, b, da, db):
    return lax.dot_general(a, b, (((da,), (db,)), ((), ())), preferred_element_type=F32)


def dot(a, b):
    ah, al = halves(a)
    bh, bl = halves(b)
    return contract(ah, bh, 1, 0) + (contract(ah, bl, 1, 0) + contract(al, bh, 1, 0))


def dot_tn(a, b):
    return dot(jnp.transpose(a), b)


def dot_nt(a, b):
    return contract(a, b, 1, 1)


def inverse_unit_triangular(strict, row, col):
    width = strict.shape[0]
    identity = (row == col).astype(F32)
    size = 1
    inverse = identity
    while size < width:
        pair = (row // (2 * size) == col // (2 * size)) & (row // size != col // size)
        off = jnp.where(pair, strict, 0.0)
        if size == 1:
            inverse = inverse - off
        else:
            inverse = inverse - dot(inverse, dot(off, inverse))
        size *= 2
    return inverse


def delta_kernel(tokens_ref, scalars_ref, reach_ref, own_ref, maps_ref, *, width):
    length = tokens_ref.shape[0]
    count = length // width
    row = lax.broadcasted_iota(jnp.int32, (width, width), 0)
    col = lax.broadcasted_iota(jnp.int32, (width, width), 1)
    eye = row == col
    identity = eye.astype(F32)
    blocks = []
    for n in range(count):
        at = pl.ds(n * width, width)
        q = tokens_ref[at, 0:DK]
        k = tokens_ref[at, DK : 2 * DK]
        v = tokens_ref[at, 2 * DK : 3 * DK].astype(F32)
        qf = q.astype(F32)
        kf = k.astype(F32)
        kk = dot_nt(k, k)
        qk = dot_nt(q, k)
        diagonal = jnp.where(eye, kk, 0.0)
        key_col = lax.rsqrt(jnp.sum(kf * kf, axis=1, keepdims=True) + EPS)
        key_row = lax.rsqrt(jnp.sum(diagonal, axis=0, keepdims=True) + EPS)
        query_col = lax.rsqrt(jnp.sum(qf * qf, axis=1, keepdims=True) + EPS) * DK ** (-0.5)
        kk = kk * key_col * key_row
        qk = qk * query_col * key_row
        keys = kf * key_col
        queries = qf * query_col
        across = scalars_ref[:, at]
        down = jnp.transpose(across)
        pieces = []
        for d in range(2):
            inside = (col <= row) if d == 0 else (col >= row)
            strict_mask = inside & ~eye
            ld_row = across[d : d + 1]
            ld_col = down[:, d : d + 1]
            beta = down[:, 2 + d : 3 + d]
            cum_col = jnp.sum(jnp.where(inside, ld_row, 0.0), axis=1, keepdims=True)
            sooner = (row <= col) if d == 0 else (row >= col)
            cum_row = jnp.sum(jnp.where(sooner, ld_col, 0.0), axis=0, keepdims=True)
            total = jnp.sum(ld_row, axis=1, keepdims=True)
            decay = jnp.exp(jnp.where(inside, cum_col - cum_row, -1e30))
            strict = jnp.where(strict_mask, kk * decay * beta, 0.0)
            inverse = inverse_unit_triangular(strict, row, col)
            grown = jnp.exp(cum_col)
            rhs = jnp.concatenate([keys * (beta * grown), v * beta], axis=1)
            solved = dot(inverse, rhs)
            reading = dot(qk * decay, solved)
            keys_decayed = keys * jnp.exp(total - cum_col)
            carried = dot_tn(keys_decayed, solved)
            reach = queries * grown - reading[:, :DK]
            transition = identity * jnp.exp(total) - carried[:, :DK]
            pieces.append((reach, reading[:, DK:], transition, carried[:, DK:]))
        blocks.append(pieces)
    own = [None] * count
    for d in range(2):
        state = None
        order = range(count) if d == 0 else range(count - 1, -1, -1)
        for n in order:
            reach, local, transition, addition = blocks[n][d]
            if state is None:
                state = jnp.concatenate([transition, addition], axis=1)
            else:
                both = dot(jnp.concatenate([reach, transition], axis=0), state)
                reach = both[:width, :DK]
                local = local + both[:width, DK:]
                state = both[width:] + jnp.concatenate(
                    [jnp.zeros_like(addition), addition], axis=1
                )
            reach_ref[d, pl.ds(n * width, width)] = reach
            own[n] = local if own[n] is None else own[n] + local
        maps_ref[d] = state
    for n in range(count):
        own_ref[pl.ds(n * width, width)] = own[n]


def finish_kernel(place_ref, maps_ref, reach_ref, own_ref, valve_ref, gain_ref, mixed_ref):
    z = place_ref[0]
    planes = maps_ref.shape[0]
    empty = jnp.zeros((DK, own_ref.shape[1]), F32)

    def absorb(at, state):
        item = maps_ref[at]
        return dot(item[:, :DK], state) + item[:, DK:]

    ahead = lax.fori_loop(0, z, absorb, empty)
    behind = lax.fori_loop(
        0, planes - 1 - z, lambda i, state: absorb(planes - 1 - i, state), empty
    )
    o = own_ref[...] + dot(reach_ref[0], ahead) + dot(reach_ref[1], behind)
    scaled = o * lax.rsqrt(jnp.mean(o * o, axis=1, keepdims=True) + EPS) * gain_ref[...]
    valve = valve_ref[...].astype(F32)
    mixed_ref[...] = (scaled * (valve / (1.0 + jnp.exp(-valve)))).astype(BF16)


def vmem(count):
    return [pl.BlockSpec(memory_space=pltpu.VMEM)] * count


def delta_rule(tokens, scalars):
    length = tokens.shape[0]
    width = min(128, length)
    return pl.pallas_call(
        functools.partial(delta_kernel, width=width),
        out_shape=(
            jax.ShapeDtypeStruct((2, length, DK), F32),
            jax.ShapeDtypeStruct((length, DK), F32),
            jax.ShapeDtypeStruct((2, DK, 2 * DK), F32),
        ),
        in_specs=vmem(2),
        out_specs=tuple(vmem(3)),
        name="delta_rule",
    )(tokens, scalars)


def finish(place, maps, reach, own, valve, gain):
    return pl.pallas_call(
        finish_kernel,
        out_shape=jax.ShapeDtypeStruct(own.shape, BF16),
        in_specs=[pl.BlockSpec(memory_space=pltpu.SMEM)] + vmem(5),
        out_specs=pl.BlockSpec(memory_space=pltpu.VMEM),
        name="finish",
    )(place, maps, reach, own, valve, gain)


def exchange(slots, axis):
    return lax.all_to_all(slots, axis, split_axis=0, concat_axis=0, tiled=True)


def rms_rows(rows, gain):
    widened = rows.astype(F32)
    return (
        widened * lax.rsqrt(jnp.mean(widened * widened, axis=-1, keepdims=True) + EPS) * gain
    ).astype(BF16)


def to_columns(stack):
    return jnp.transpose(stack, (1, 0, 2)).reshape(stack.shape[1], -1)


def body(
    skip_pathway,
    request_vectors,
    lookup_address_matrix,
    content_vectors,
    result_valve_matrix,
    shrink_raw_signal,
    channel_shrink_speed,
    insertion_raw_signal,
    extra_shrink_spike,
    channel_scaling_vector,
    final_mapping_matrix,
    mixer_scaling_vector,
    valve_matrix,
    widening_matrix,
    temporal_kernel_entries,
    narrowing_matrix,
):
    group = lax.axis_size("p")
    planes = lax.axis_size("z")
    cores = lax.axis_size("tp")
    p = lax.axis_index("p")
    z = lax.axis_index("z")
    rows, features = skip_pathway.shape
    length = group * rows

    def spread(weight):
        parts = jnp.transpose(weight.reshape(rows_w(weight), group, -1), (1, 0, 2))
        return exchange(parts, "p").reshape(-1, parts.shape[-1])

    def rows_w(weight):
        return weight.shape[0]

    valve_rows = spread(valve_matrix)
    valve_full = lax.all_gather(valve_rows, "z", axis=0, tiled=True)
    widening_rows = spread(widening_matrix)
    widening_full = lax.all_gather(widening_rows, "z", axis=0, tiled=True)
    narrow_parts = narrowing_matrix.reshape(group, -1, narrowing_matrix.shape[1])
    narrow_cols = to_columns(exchange(narrow_parts, "p"))
    narrow_full = lax.all_gather(narrow_cols, "z", axis=1, tiled=True)

    packed = jnp.stack(
        [
            a.reshape(rows, group, DK)
            for a in (request_vectors, lookup_address_matrix, content_vectors, result_valve_matrix)
        ],
        axis=2,
    )
    packed = jnp.transpose(packed.reshape(rows, group, 4 * DK), (1, 0, 2))
    tokens = exchange(packed, "p").reshape(length, 4 * DK)
    log_decay = (
        -channel_shrink_speed[:, :, None] * jax.nn.softplus(shrink_raw_signal) + extra_shrink_spike
    )
    beta = jax.nn.sigmoid(insertion_raw_signal)
    scalars = jnp.concatenate([log_decay, beta, jnp.zeros_like(log_decay), jnp.zeros_like(beta)], axis=0)
    scalars = exchange(jnp.transpose(scalars, (1, 0, 2)), "p")
    scalars = to_columns(scalars)

    reach, own, maps = delta_rule(tokens, scalars)
    plane_ids = jnp.arange(planes).reshape(planes, 1, 1)
    outgoing = jnp.where(plane_ids > z, maps[0][None], maps[1][None])
    incoming = exchange(outgoing, "z")
    mixed = finish(
        z.reshape(1).astype(jnp.int32),
        incoming,
        reach,
        own,
        tokens[:, 3 * DK :],
        channel_scaling_vector.reshape(1, -1),
    )

    heads = to_columns(lax.all_gather(mixed, "p", axis=0))
    heads = exchange(jnp.broadcast_to(heads[None], (cores,) + heads.shape), "tp")
    projected = jnp.dot(
        to_columns(heads), final_mapping_matrix, preferred_element_type=F32
    )
    skip = exchange(jnp.broadcast_to(skip_pathway[None], (group, rows, features)), "p")
    middle = (skip.reshape(length, features).astype(F32) + projected).astype(BF16)
    full_rows = to_columns(exchange(jnp.broadcast_to(middle[None], (cores,) + middle.shape), "tp"))
    normed = rms_rows(full_rows, mixer_scaling_vector)

    gate = jnp.dot(normed, valve_full, preferred_element_type=F32).astype(BF16)
    up = jnp.dot(normed, widening_full, preferred_element_type=F32)
    size = planes
    before = lax.ppermute(gate[-1:], "z", [(i, i + 1) for i in range(size - 1)])
    after = lax.ppermute(gate[:1], "z", [(i + 1, i) for i in range(size - 1)])
    padded = jnp.concatenate([before, gate, after], axis=0).astype(F32)
    units = gate.shape[1]
    taps = lax.dynamic_slice_in_dim(temporal_kernel_entries, p * units, units, axis=1)
    convolved = padded[:-2] * taps[0] + padded[1:-1] * taps[1] + padded[2:] * taps[2]
    hidden = (jax.nn.silu(convolved) * up).astype(BF16)
    terms = jnp.dot(hidden, narrow_full, preferred_element_type=F32).astype(BF16)
    terms = jnp.transpose(terms.reshape(group, rows, cores, features), (0, 2, 1, 3))
    terms = exchange(terms.reshape(group * cores, rows, features), ("p", "tp"))
    down = jnp.sum(terms.astype(F32), axis=0)
    mine = lax.dynamic_slice_in_dim(middle, p * rows, rows, axis=0)
    return (mine.astype(F32) + down).astype(BF16)


def solution(mesh):
    def layer(*args):
        cores = mesh.shape["tp"]
        group = args[5].shape[1] // cores
        split = Mesh(mesh.devices.reshape(-1, group, cores), ("z", "p", "tp"))
        sp = ("z", "p")
        return jax.shard_map(
            body,
            mesh=split,
            in_specs=(
                P(sp, "tp"),
                P(sp, "tp"),
                P(sp, "tp"),
                P(sp, "tp"),
                P(sp, "tp"),
                P(None, "tp", sp),
                P(None, "tp"),
                P(None, "tp", sp),
                P(None, "tp", sp),
                P(),
                P(None, "tp"),
                P(),
                P(sp, "tp"),
                P(sp, "tp"),
                P(None, "tp"),
                P("tp", sp),
            ),
            out_specs=P(sp, "tp"),
            check_vma=False,
        )(*args)

    return layer
```

time: 576 us -> 259 us (0.45)
  waiting for transfers between devices: 275 us -> 58.7 us
  starting transfers between devices: 124 us -> 18.2 us
  matrix products: 122 us -> 16.4 us
  blocking collectives: 4.18 us -> 90.3 us
  Pallas kernels: 0 us -> 26.5 us
    ppermute x32 -> x2, waiting for transfers between devices: 196 us -> 4.55 us  [the longest x1 4.54 us: body(): after = lax.ppermute(gate[:1], 'z', [(i + 1, i) for i in range(size - 1)])]
    ppermute x32 -> x2, starting transfers between devices: 124 us -> 2.58 us  [the longest x1 1.29 us: body(): after = lax.ppermute(gate[:1], 'z', [(i + 1, i) for i in range(size - 1)])]
    dot_general x89 -> x3, matrix products: 122 us -> 16.4 us  [the longest x1 8.71 us: body(): jnp.dot(hidden, narrow_full, preferred_element_type=F32).astype(BF16)]
    all_to_all x0 -> x6, blocking collectives: none -> 79.3 us  [exchange(): return lax.all_to_all(slots, axis, split_axis=0, concat_axis=0, tiled=True)]
    all_gather x3, waiting for transfers between devices: 70.8 us -> 26.8 us  [the longest x1 26.8 us: body(): narrow_full = lax.all_gather(narrow_cols, 'z', axis=1, tiled=True)]
    all_to_all x0 -> x4, waiting for transfers between devices: none -> 27.3 us  [exchange(): return lax.all_to_all(slots, axis, split_axis=0, concat_axis=0, tiled=True)]
    pallas_call x0 -> x2, Pallas kernels: none -> 26.5 us  [the longest x1 23.5 us: delta_rule(): pl.pallas_call(functools.partial(delta_kernel, width=width), out_shape=(j...]
    all_to_all x0 -> x4, starting transfers between devices: none -> 15.4 us  [exchange(): return lax.all_to_all(slots, axis, split_axis=0, concat_axis=0, tiled=True)]
  transfers between devices with their start and end apart: 36 -> 9, of which waited for: 34 -> 4; matrix products, arithmetic and copies ran while one was open for 24% -> 10% of each run, Pallas kernels for 0% -> 10%
where the time goes in v1:
time: 259 us; the launch traced here: 258 us
  blocking collectives  90.3 us (35%)
  waiting for transfers between devices  58.7 us (23%)
  Pallas kernels  26.5 us (10%)
  local copies, waits for them, and re-layouts  25.5 us (10%)
  starting transfers between devices  18.2 us (7%)
  matrix products  16.4 us (6%)
  between operations  13.4 us (5%)
  other arithmetic  8.79 us (3%)
    all_to_all x6, blocking collectives, exchange(): return lax.all_to_all(slots, axis, split_axis=0, concat_axis=0, tiled=True)  79.3 us
    all_to_all x4, waiting for transfers between devices, exchange(): return lax.all_to_all(slots, axis, split_axis=0, concat_axis=0, tiled=True)  27.3 us
    all_gather x1, waiting for transfers between devices, body(): narrow_full = lax.all_gather(narrow_cols, 'z', axis=1, tiled=True)  26.8 us
    pallas_call x1, Pallas kernels, delta_rule(): pl.pallas_call(functools.partial(delta_kernel, width=width), out_shape=(j...  23.5 us
    all_to_all x4, starting transfers between devices, exchange(): return lax.all_to_all(slots, axis, split_axis=0, concat_axis=0, tiled=True)  15.4 us
    all_gather x1, blocking collectives, body(): heads = to_columns(lax.all_gather(mixed, 'p', axis=0))  11 us
    dot_general x1, matrix products, body(): jnp.dot(hidden, narrow_full, preferred_element_type=F32).astype(BF16)  8.71 us
    reshape x2, local copies, waits for them, and re-layouts, body(): terms.reshape(group, rows, cores, features)  8.05 us
  transfers between devices with their start and end apart: 9, of which 4 were waited for; matrix products, arithmetic and copies ran while one was open for 10% of the time, Pallas kernels for 10%

profile of v1, /device:TPU:0, one launch (start us, length us, event | category | flops | bytes accessed | tf_op | source)
XLA Modules:
  0.0 257.8 jit_solution(16278481964983617024)
XLA Ops:
  6.5 1.6 copy.31
  8.1 14.9 %all_to_all.50 = bf16[4,128,640]{1,2,0:T(8,128)(2,1)S(1)} all-to-all(bf16[4,128,640]{1,2,0:T(8,128)(2,1)S(1)} %bitcast.60), channel_id=1, replica_groups=mesh['z'=4,'p'=4,'tp'=2] {'p'}, dimensions={0} | all-to-all | bytes 1310720 | tf_op jit(solution)/shard_map/all_to_all | solution.py:177
  24.2 1.4 copy.33
  25.7 11.1 %all_to_all.51 = bf16[4,128,640]{1,2,0:T(8,128)(2,1)S(1)} all-to-all(bf16[4,128,640]{1,2,0:T(8,128)(2,1)S(1)} %bitcast.61), channel_id=1, replica_groups=mesh['z'=4,'p'=4,'tp'=2] {'p'}, dimensions={0} | all-to-all | bytes 1310720 | tf_op jit(solution)/shard_map/all_to_all | solution.py:177
  38.8 3.3 %all-to-all-start.2 = ((f32[4,8,128]{2,1,0:T(8,128)}), f32[4,8,128]{2,1,0:T(8,128)S(1)}, u32[]{:S(2)}, u32[]{:S(2)}) async-start(f32[4,8,128]{2,1,0:T(8,128)} %maximum_bitcast_fusion), calls=%async_computation.2 | async-start | bytes 32768 | tf_op jit(solution)/shard_map/all_to_all | solution.py:177
  46.8 10.5 %all_to_all.52 = bf16[4,128,512]{2,1,0:T(8,128)(2,1)} all-to-all(bf16[4,128,512]{2,1,0:T(8,128)(2,1)S(1)} %bitcast.64), channel_id=1, replica_groups=mesh['z'=4,'p'=4,'tp'=2] {'p'}, dimensions={0} | all-to-all | bytes 1048576 | tf_op jit(solution)/shard_map/all_to_all | solution.py:177
  57.3 3.5 %all-to-all-start.8 = ((bf16[4,640,128]{2,1,0:T(8,128)(2,1)}), bf16[4,640,128]{2,1,0:T(8,128)(2,1)S(1)}, u32[]{:S(2)}, u32[]{:S(2)}) async-start(bf16[4,640,128]{2,1,0:T(8,128)(2,1)} %bitcast.66), calls=%async_computation.8 | async-start | bytes 1310720 | tf_op jit(solution)/shard_map/all_to_all | solution.py:177
  61.0 23.5 %delta_rule.1 = (f32[2,512,128]{2,1,0:T(8,128)}, f32[512,128]{1,0:T(8,128)}, f32[2,128,256]{2,1,0:T(8,128)}) custom-call(bf16[512,512]{1,0:T(8,128)(2,1)} %bitcast.54, f32[8,512]{1,0:T(8,128)} %bitcast.67), custom_call_target="tpu_custom_call" | custom-call | tf_op jit(solution)/shard_map/delta_rule/pallas_call | solution.py:153
  85.6 1.1 copy.35
  86.9 32.8 %all_to_all.53.maps_ref = f32[4,128,256]{2,1,0:T(8,128)} all-to-all(f32[4,128,256]{2,1,0:T(8,128)S(1)} %broadcast_select_fusion), channel_id=1, replica_groups=mesh['z'=4,'p'=4,'tp'=2] {'z'}, dimensions={0} | all-to-all | bytes 1048576 | tf_op jit(solution)/shard_map/all_to_all | solution.py:177
  120.7 4.3 %all-to-all-start = ((bf16[4,128,1024]{2,1,0:T(8,128)(2,1)}), bf16[4,128,1024]{2,1,0:T(8,128)(2,1)}, u32[]{:S(2)}, u32[]{:S(2)}) async-start(bf16[4,128,1024]{2,1,0:T(8,128)(2,1)} %broadcast_in_dim.50), calls=%async_computation | async-start | bytes 2097152 | tf_op jit(solution)/shard_map/all_to_all | solution.py:177
  125.0 1.6 slice.44.valve_ref
  126.6 3.0 %finish.1 = bf16[512,128]{1,0:T(8,128)(2,1)} custom-call(s32[1]{0:T(128)} %bitcast.1.place_ref, f32[4,128,256]{2,1,0:T(8,128)} %all_to_all.53.maps_ref, f32[2,512,128]{2,1,0:T(8,128)} %get-tuple-element.9.reach_ref, f32[512,128]{1,0:T(8,128)} %get-tuple-element.10.own_ref, bf16[512,128]{1,0:T(8,128)(2,1)} %slice.44.valve_ref, f32[1,128]{1,0:T(1,128)} %bitcast.68), custom_call_target="tpu_custom_call" | custom-call | tf_op jit(solution)/shard_map/finish/pallas_call | solution.py:167
  129.6 11.0 %all-gather = bf16[2048,128]{1,0:T(8,128)(2,1)S(1)} all-gather(bf16[512,128]{1,0:T(8,128)(2,1)} %finish.1), channel_id=2, replica_groups=mesh['z'=4,'p'=4,'tp'=2] {'p'}, dimensions={0}, use_global_device_ids=true | all-gather | bytes 655360 | tf_op jit(solution)/shard_map/all_gather | solution.py:262
  140.8 4.6 %all_to_all.54 = bf16[2,512,512]{1,2,0:T(8,128)(2,1)S(1)} all-to-all(bf16[2,512,512]{1,2,0:T(8,128)(2,1)S(1)} %broadcast_in_dim.57), channel_id=1, replica_groups=mesh['z'=4,'p'=4,'tp'=2] {'tp'}, dimensions={0} | all-to-all | bytes 2097152 | tf_op jit(solution)/shard_map/all_to_all | solution.py:177
  145.4 3.5 %fusion.2 = bf16[512,1024]{1,0:T(8,128)(2,1)} fusion(bf16[512,1024]{1,0:T(8,128)(2,1)} %bitcast.28, bf16[512,1024]{0,1:T(8,128)(2,1)S(1)} %bitcast.65, bf16[1024,1024]{1,0:T(8,128)(2,1)S(1)} %copy-done), kind=kOutput, calls=%fused_computation.7 | convolution fusion | flops 1075314688 | bytes 5242880 | tf_op jit(solution)/shard_map/dot_general | solution.py:264
  148.9 1.5 copy.30
  150.6 5.4 %all_to_all.55 = bf16[2,512,1024]{1,2,0:T(8,128)(2,1)S(1)} all-to-all(bf16[2,512,1024]{1,2,0:T(8,128)(2,1)S(1)} %broadcast_in_dim.58), channel_id=1, replica_groups=mesh['z'=4,'p'=4,'tp'=2] {'tp'}, dimensions={0} | all-to-all | bytes 4194304 | tf_op jit(solution)/shard_map/all_to_all | solution.py:177
  156.7 1.9 fusion.1
  158.6 4.2 %convolution_convert_fusion.1 = bf16[512,640]{1,0:T(8,128)(2,1)S(1)} fusion(bf16[512,2048]{0,1:T(8,128)(2,1)} %fusion.1, bf16[2048,640]{1,0:T(8,128)(2,1)} %all-gather.5.cloned.1.call-done), kind=kOutput, calls=%fused_computation.10 | convolution fusion | flops 1342504960 | bytes 5373952 | tf_op jit(solution)/shard_map/dot_general | solution.py:272
  163.7 1.3 collective-permute-start
  165.0 1.3 collective-permute-start.1
  167.2 4.5 %collective-permute-done.1 = bf16[1,640]{1,0:T(2,128)(2,1)S(1)} collective-permute-done((bf16[1,640]{1,0:T(2,128)(2,1)S(1)}, bf16[1,640]{1,0:T(2,128)(2,1)S(1)}, u32[]{:S(2)}, u32[]{:S(2)}) %collective-permute-start.1) | collective-permute-done | bytes 1312 | tf_op jit(solution)/shard_map/ppermute | solution.py:276
  171.8 1.2 maximum_convert_fusion
  173.0 26.8 %all-gather.9.cloned.1.call-done = bf16[640,2048]{0,1:T(8,128)(2,1)} async-done(((bf16[640,512]{0,1:T(8,128)(2,1)}), bf16[640,2048]{0,1:T(8,128)(2,1)}) %all-gather.9.cloned.1.call-update) | async-done | bytes 2621456 | tf_op jit(solution)/shard_map/all_gather | solution.py:230
  199.8 8.7 %convolution_convert_fusion = bf16[512,2048]{1,0:T(8,128)(2,1)} fusion(bf16[640,2048]{0,1:T(8,128)(2,1)} %all-gather.9.cloned.1.call-done, bf16[512,2048]{0,1:T(8,128)(2,1)} %fusion.1, bf16[2048,640]{1,0:T(8,128)(2,1)} %all-gather.7.cloned.1.call-done, f32[514,640]{1,0:T(8,128)S(1)} %maximum_convert_fusion, f32[640]{0:T(1024)S(1)} %get-tuple-element.13, ...), kind=kOutput, calls=%fused_computation.5 | convolution fusion | flops 2689007616 | bytes 13381632 | tf_op jit(solution)/shard_map/dot_general | solution.py:282
  208.5 4.5 %reshape.80 = bf16[4,128,2,1024]{3,2,1,0:T(2,128)(2,1)} reshape(bf16[512,2048]{1,0:T(8,128)(2,1)} %convolution_convert_fusion) | data formatting | bytes 4194304 | tf_op jit(solution)/shard_map/reshape | solution.py:283
  213.0 3.5 %copy.36 = bf16[4,128,2,1024]{3,1,2,0:T(8,128)(2,1)} copy(bf16[4,128,2,1024]{3,2,1,0:T(2,128)(2,1)} %reshape.80) | data formatting | bytes 4194304 | tf_op jit(solution)/shard_map/reshape | solution.py:283
  216.6 4.4 %all-to-all-start.9 = ((bf16[8,128,1024]{2,1,0:T(8,128)(2,1)}), bf16[8,128,1024]{2,1,0:T(8,128)(2,1)}, u32[]{:S(2)}, u32[]{:S(2)}) async-start(bf16[8,128,1024]{2,1,0:T(8,128)(2,1)} %bitcast.53), calls=%async_computation.9 | async-start | bytes 4194304 | tf_op jit(solution)/shard_map/all_to_all | solution.py:177
  220.9 26.6 %all-to-all-done.9 = bf16[8,128,1024]{2,1,0:T(8,128)(2,1)} async-done(((bf16[8,128,1024]{2,1,0:T(8,128)(2,1)}), bf16[8,128,1024]{2,1,0:T(8,128)(2,1)}, u32[]{:S(2)}, u32[]{:S(2)}) %all-to-all-start.9) | async-done | bytes 2097184 | tf_op jit(solution)/shard_map/all_to_all | solution.py:177
  247.6 2.0 convert_reduce_fusion
  249.6 1.7 add_convert_fusion
  (60 shorter events, 13.2 us)
Async XLA Ops:
  6.5 138.9 %copy-start = (bf16[1024,1024]{1,0:T(8,128)(2,1)S(1)}, bf16[1024,1024]{1,0:T(8,128)(2,1)}, u32[]{:S(2)}) copy-start(bf16[1024,1024]{1,0:T(8,128)(2,1)} %param.26) | copy-start | bytes 6291460
  6.5 152.1 %all-gather.5.cloned.1.call-start = ((), (), s32[]{:S(2)}) async-start(), calls=%async_computation.10 | async-start | bytes 3276800 | tf_op jit(solution)/shard_map/all_gather | solution.py:225
  24.1 13.8 %copy-start.9 = (f32[2,4]{1,0:T(2,128)S(1)}, f32[2,4]{1,0:T(2,128)}, u32[]{:S(2)}) copy-start(f32[2,4]{1,0:T(2,128)} %param.22) | copy-start | bytes 100
  24.1 13.8 %copy-start.6 = (f32[2,4,128]{2,1,0:T(4,128)S(1)}, f32[2,4,128]{2,1,0:T(4,128)}, u32[]{:S(2)}) copy-start(f32[2,4,128]{2,1,0:T(4,128)} %param.24) | copy-start | bytes 12292
  24.2 13.8 %copy-start.7 = (f32[2,4,128]{2,1,0:T(4,128)S(1)}, f32[2,4,128]{2,1,0:T(4,128)}, u32[]{:S(2)}) copy-start(f32[2,4,128]{2,1,0:T(4,128)} %param.21) | copy-start | bytes 12292
  24.2 13.9 %copy-start.8 = (f32[2,4,128]{2,1,0:T(4,128)S(1)}, f32[2,4,128]{2,1,0:T(4,128)}, u32[]{:S(2)}) copy-start(f32[2,4,128]{2,1,0:T(4,128)} %param.23) | copy-start | bytes 12292
  24.2 17.9 %copy-start.3 = (bf16[128,512]{1,0:T(8,128)(2,1)S(1)}, bf16[128,512]{1,0:T(8,128)(2,1)}, u32[]{:S(2)}) copy-start(bf16[128,512]{1,0:T(8,128)(2,1)} %param.17) | copy-start | bytes 393220
  24.2 148.8 %all-gather.7.cloned.1.call-start = ((), (), s32[]{:S(2)}) async-start(), calls=%async_computation.11 | async-start | bytes 3276800 | tf_op jit(solution)/shard_map/all_gather | solution.py:227
  38.8 7.9 %all-to-all-start.2 = ((f32[4,8,128]{2,1,0:T(8,128)}), f32[4,8,128]{2,1,0:T(8,128)S(1)}, u32[]{:S(2)}, u32[]{:S(2)}) async-start(f32[4,8,128]{2,1,0:T(8,128)} %maximum_bitcast_fusion), calls=%async_computation.2 | async-start | bytes 32768 | tf_op jit(solution)/shard_map/all_to_all | solution.py:177
  46.8 14.3 %copy-start.4 = (f32[4,8,128]{2,1,0:T(8,128)}, f32[4,8,128]{2,1,0:T(8,128)S(1)}, u32[]{:S(2)}) copy-start(f32[4,8,128]{2,1,0:T(8,128)S(1)} %all-to-all-done.2) | copy-start | bytes 49156
  57.3 28.3 %all-to-all-start.8 = ((bf16[4,640,128]{2,1,0:T(8,128)(2,1)}), bf16[4,640,128]{2,1,0:T(8,128)(2,1)S(1)}, u32[]{:S(2)}, u32[]{:S(2)}) async-start(bf16[4,640,128]{2,1,0:T(8,128)(2,1)} %bitcast.66), calls=%async_computation.8 | async-start | bytes 1310720 | tf_op jit(solution)/shard_map/all_to_all | solution.py:177
  60.8 139.0 %all-gather.9.cloned.1.call-start = ((), (), s32[]{:S(2)}) async-start(), calls=%async_computation.12 | async-start | bytes 3276800 | tf_op jit(solution)/shard_map/all_gather | solution.py:230
  84.6 35.1 %copy-start.2 = (bf16[128,1024]{1,0:T(8,128)(2,1)S(1)}, bf16[128,1024]{1,0:T(8,128)(2,1)}, u32[]{:S(2)}) copy-start(bf16[128,1024]{1,0:T(8,128)(2,1)} %param.16) | copy-start | bytes 786436
  120.7 20.0 %all-to-all-start = ((bf16[4,128,1024]{2,1,0:T(8,128)(2,1)}), bf16[4,128,1024]{2,1,0:T(8,128)(2,1)}, u32[]{:S(2)}, u32[]{:S(2)}) async-start(bf16[4,128,1024]{2,1,0:T(8,128)(2,1)} %broadcast_in_dim.50), calls=%async_computation | async-start | bytes 2097152 | tf_op jit(solution)/shard_map/all_to_all | solution.py:177
  156.0 0.7 copy-start.5
  162.9 0.8 copy-start.1
  163.7 3.5 %collective-permute-start = (bf16[1,640]{1,0:T(2,128)(2,1)S(1)}, bf16[1,640]{1,0:T(2,128)(2,1)S(1)}, u32[]{:S(2)}, u32[]{:S(2)}) collective-permute-start(bf16[1,640]{1,0:T(2,128)(2,1)S(1)} %get-tuple-element.14), channel_id=1, source_target_pairs={{0,8},{8,16},{16,24},{1,9},{9,17},{17,25},{2,10},{10,18},{18,26},{... | collective-permute-start | bytes 3848 | tf_op jit(solution)/shard_map/ppermute | solution.py:275
  165.0 6.8 %collective-permute-start.1 = (bf16[1,640]{1,0:T(2,128)(2,1)S(1)}, bf16[1,640]{1,0:T(2,128)(2,1)S(1)}, u32[]{:S(2)}, u32[]{:S(2)}) collective-permute-start(bf16[1,640]{1,0:T(2,128)(2,1)S(1)} %get-tuple-element.15), channel_id=1, source_target_pairs={{8,0},{16,8},{24,16},{9,1},{17,9},{25,17},{10,2},{18,10},{26,18},{... | collective-permute-start | bytes 3848 | tf_op jit(solution)/shard_map/ppermute | solution.py:276
  216.6 31.0 %all-to-all-start.9 = ((bf16[8,128,1024]{2,1,0:T(8,128)(2,1)}), bf16[8,128,1024]{2,1,0:T(8,128)(2,1)}, u32[]{:S(2)}, u32[]{:S(2)}) async-start(bf16[8,128,1024]{2,1,0:T(8,128)(2,1)} %bitcast.53), calls=%async_computation.9 | async-start | bytes 4194304 | tf_op jit(solution)/shard_map/all_to_all | solution.py:177
Sparse Core Ops, SparseCore 0:
  24.3 54.4 all-gather.4
  80.4 63.9 all-gather.6
  145.9 53.8 all-gather.8

commit v2 on v1

--- a/solution.py
+++ b/solution.py
@@ -173,6 +173,64 @@
     )(place, maps, reach, own, valve, gain)
 
 
+def copy_kernel(*refs, moves, sources):
+    inputs, output, semaphores = refs[:sources], refs[sources], refs[sources + 1]
+    copies = []
+    for index, (source, take, put) in enumerate(moves):
+        copies.append(
+            pltpu.make_async_copy(
+                inputs[source].at[take], output.at[put], semaphores.at[index]
+            )
+        )
+    for copy in copies:
+        copy.start()
+    for copy in copies:
+        copy.wait()
+
+
+def rearrange(arrays, shape, moves, name):
+    count = len(arrays)
+    return pl.pallas_call(
+        functools.partial(copy_kernel, moves=tuple(moves), sources=count),
+        out_shape=jax.ShapeDtypeStruct(shape, arrays[0].dtype),
+        in_specs=[pl.BlockSpec(memory_space=pl.ANY)] * count,
+        out_specs=pl.BlockSpec(memory_space=pl.ANY),
+        scratch_shapes=[pltpu.SemaphoreType.DMA((len(moves),))],
+        name=name,
+    )(*arrays)
+
+
+def span(index, size):
+    return pl.ds(index * size, size)
+
+
+ALL = slice(None)
+
+
+def down_kernel(hidden_ref, weight_ref, out_ref):
+    out_ref[0] = jnp.dot(
+        hidden_ref[...], weight_ref[...], preferred_element_type=F32
+    ).astype(BF16)
+
+
+def down_product(hidden, weight, cores):
+    length, units = hidden.shape
+    features = weight.shape[1] // cores
+    tile = min(512, features)
+    steps = features // tile
+    return pl.pallas_call(
+        down_kernel,
+        grid=(cores, steps),
+        out_shape=jax.ShapeDtypeStruct((cores, length, features), BF16),
+        in_specs=[
+            pl.BlockSpec((length, units), lambda c, n: (0, 0)),
+            pl.BlockSpec((units, tile), lambda c, n: (0, c * steps + n)),
+        ],
+        out_specs=pl.BlockSpec((1, length, tile), lambda c, n: (c, 0, n)),
+        name="down",
+    )(hidden, weight)
+
+
 def exchange(slots, axis):
     return lax.all_to_all(slots, axis, split_axis=0, concat_axis=0, tiled=True)
 
@@ -214,29 +272,37 @@
     rows, features = skip_pathway.shape
     length = group * rows
 
-    def spread(weight):
-        parts = jnp.transpose(weight.reshape(rows_w(weight), group, -1), (1, 0, 2))
-        return exchange(parts, "p").reshape(-1, parts.shape[-1])
-
-    def rows_w(weight):
-        return weight.shape[0]
-
-    valve_rows = spread(valve_matrix)
-    valve_full = lax.all_gather(valve_rows, "z", axis=0, tiled=True)
-    widening_rows = spread(widening_matrix)
-    widening_full = lax.all_gather(widening_rows, "z", axis=0, tiled=True)
-    narrow_parts = narrowing_matrix.reshape(group, -1, narrowing_matrix.shape[1])
-    narrow_cols = to_columns(exchange(narrow_parts, "p"))
-    narrow_full = lax.all_gather(narrow_cols, "z", axis=1, tiled=True)
-
-    packed = jnp.stack(
-        [
-            a.reshape(rows, group, DK)
-            for a in (request_vectors, lookup_address_matrix, content_vectors, result_valve_matrix)
-        ],
-        axis=2,
-    )
-    packed = jnp.transpose(packed.reshape(rows, group, 4 * DK), (1, 0, 2))
+    depth = valve_matrix.shape[0]
+    units = valve_matrix.shape[1] // group
+    moves = [
+        (w, (ALL, span(j, units)), (j, w)) for j in range(group) for w in range(2)
+    ]
+    pair = rearrange(
+        (valve_matrix, widening_matrix), (group, 2, depth, units), moves, "pack_pair"
+    )
+    pair = exchange(pair, "p")
+    moves = [(0, (j, w), (w, j)) for j in range(group) for w in range(2)]
+    pair = rearrange((pair,), (2, group, depth, units), moves, "place_pair")
+    pair = pair.reshape(2, group * depth, units)
+    pair = lax.all_gather(pair, "z", axis=1, tiled=True)
+    width = narrowing_matrix.shape[1]
+    narrow = exchange(narrowing_matrix.reshape(group, units, width), "p")
+    if width % 128 == 0:
+        moves = [(0, (j,), (ALL, span(j, width))) for j in range(group)]
+        narrow = rearrange((narrow,), (units, group * width), moves, "place_narrow")
+    else:
+        narrow = to_columns(narrow)
+    narrow_full = lax.all_gather(narrow, "z", axis=1, tiled=True)
+
+    moves = [
+        (a, (ALL, span(j, DK)), (j, ALL, span(a, DK))) for j in range(group) for a in range(4)
+    ]
+    packed = rearrange(
+        (request_vectors, lookup_address_matrix, content_vectors, result_valve_matrix),
+        (group, rows, 4 * DK),
+        moves,
+        "pack_tokens",
+    )
     tokens = exchange(packed, "p").reshape(length, 4 * DK)
     log_decay = (
         -channel_shrink_speed[:, :, None] * jax.nn.softplus(shrink_raw_signal) + extra_shrink_spike
@@ -269,19 +335,17 @@
     full_rows = to_columns(exchange(jnp.broadcast_to(middle[None], (cores,) + middle.shape), "tp"))
     normed = rms_rows(full_rows, mixer_scaling_vector)
 
-    gate = jnp.dot(normed, valve_full, preferred_element_type=F32).astype(BF16)
-    up = jnp.dot(normed, widening_full, preferred_element_type=F32)
-    size = planes
-    before = lax.ppermute(gate[-1:], "z", [(i, i + 1) for i in range(size - 1)])
-    after = lax.ppermute(gate[:1], "z", [(i + 1, i) for i in range(size - 1)])
+    gate = jnp.dot(normed, pair[0], preferred_element_type=F32).astype(BF16)
+    up = jnp.dot(normed, pair[1], preferred_element_type=F32)
+    before = lax.ppermute(gate[-1:], "z", [(i, i + 1) for i in range(planes - 1)])
+    after = lax.ppermute(gate[:1], "z", [(i + 1, i) for i in range(planes - 1)])
     padded = jnp.concatenate([before, gate, after], axis=0).astype(F32)
-    units = gate.shape[1]
     taps = lax.dynamic_slice_in_dim(temporal_kernel_entries, p * units, units, axis=1)
     convolved = padded[:-2] * taps[0] + padded[1:-1] * taps[1] + padded[2:] * taps[2]
     hidden = (jax.nn.silu(convolved) * up).astype(BF16)
-    terms = jnp.dot(hidden, narrow_full, preferred_element_type=F32).astype(BF16)
-    terms = jnp.transpose(terms.reshape(group, rows, cores, features), (0, 2, 1, 3))
-    terms = exchange(terms.reshape(group * cores, rows, features), ("p", "tp"))
+    terms = down_product(hidden, narrow_full, cores)
+    terms = jnp.sum(exchange(terms, "tp").astype(F32), axis=0).astype(BF16)
+    terms = exchange(terms.reshape(group, rows, features), "p")
     down = jnp.sum(terms.astype(F32), axis=0)
     mine = lax.dynamic_slice_in_dim(middle, p * rows, rows, axis=0)
     return (mine.astype(F32) + down).astype(BF16)

time: 259 us -> 320 us (1.24)
  Pallas kernels: 26.5 us -> 152 us
  blocking collectives: 90.3 us -> 53.3 us
  local copies, waits for them, and re-layouts: 25.5 us -> 6.83 us
  waiting for transfers between devices: 58.7 us -> 44.4 us
  starting transfers between devices: 18.2 us -> 26.1 us
    pallas_call x0 -> x5, Pallas kernels: none -> 125 us  [the longest x4 120 us: rearrange(): pl.pallas_call(functools.partial(copy_kernel, moves=tuple(moves), sources...]
    all_to_all x6 -> x4, blocking collectives: 79.3 us -> 41.5 us  [exchange(): return lax.all_to_all(slots, axis, split_axis=0, concat_axis=0, tiled=True)]
    all_gather x3 -> x2, waiting for transfers between devices: 26.8 us -> 11.1 us  [the longest x1 11.1 us: body(): narrow_full = lax.all_gather(narrow, 'z', axis=1, tiled=True)]
    reshape x3 -> x0, local copies, waits for them, and re-layouts: 8.25 us -> none  [the longest x2 8.05 us: body(): terms.reshape(group, rows, cores, features)]
    all_to_all x4 -> x6, starting transfers between devices: 15.4 us -> 23.5 us  [exchange(): return lax.all_to_all(slots, axis, split_axis=0, concat_axis=0, tiled=True)]
    unnamed x22, local copies, waits for them, and re-layouts: 4.05 us -> 0.04 us
    reduce_sum x0 -> x1, other arithmetic: none -> 3.33 us  [body(): terms = jnp.sum(exchange(terms, 'tp').astype(F32), axis=0).astype(BF16)]
    another operation x5 -> x0, local copies, waits for them, and re-layouts: 3.27 us -> none  [body(): jnp.stack([a.reshape(rows, group, DK) for a in (request_vectors, lookup_a...]
  transfers between devices with their start and end apart: 9 -> 10, of which waited for: 4 -> 5; matrix products, arithmetic and copies ran while one was open for 10% -> 8% of each run, Pallas kernels for 10% -> 20%
where the time goes in v2:
time: 320 us; the launch traced here: 319 us
  Pallas kernels  152 us (48%)
  blocking collectives  53.3 us (17%)
  waiting for transfers between devices  44.4 us (14%)
  starting transfers between devices  26.1 us (8%)
  between operations  13.7 us (4%)
  matrix products  13.3 us (4%)
  other arithmetic  9.5 us (3%)
  local copies, waits for them, and re-layouts  6.83 us (2%)
    pallas_call x4, Pallas kernels, rearrange(): pl.pallas_call(functools.partial(copy_kernel, moves=tuple(moves), sources...  120 us
    all_to_all x4, blocking collectives, exchange(): return lax.all_to_all(slots, axis, split_axis=0, concat_axis=0, tiled=True)  41.5 us
    all_to_all x6, waiting for transfers between devices, exchange(): return lax.all_to_all(slots, axis, split_axis=0, concat_axis=0, tiled=True)  29.9 us
    all_to_all x6, starting transfers between devices, exchange(): return lax.all_to_all(slots, axis, split_axis=0, concat_axis=0, tiled=True)  23.5 us
    pallas_call x1, Pallas kernels, delta_rule(): pl.pallas_call(functools.partial(delta_kernel, width=width), out_shape=(j...  23.5 us
    all_gather x1, blocking collectives, body(): heads = to_columns(lax.all_gather(mixed, 'p', axis=0))  11.8 us
    all_gather x1, waiting for transfers between devices, body(): narrow_full = lax.all_gather(narrow, 'z', axis=1, tiled=True)  11.1 us
  transfers between devices with their start and end apart: 10, of which 5 were waited for; matrix products, arithmetic and copies ran while one was open for 8% of the time, Pallas kernels for 20%

profile of v2, /device:TPU:0, one launch (start us, length us, event | category | flops | bytes accessed | tf_op | source)
XLA Modules:
  0.0 318.7 jit_solution(16643674330319600417)
XLA Ops:
  6.5 40.9 %pack_pair.1 = bf16[4,2,128,640]{3,2,1,0:T(8,128)(2,1)} custom-call(bf16[128,2560]{1,0:T(8,128)(2,1)} %refs_0_.3, bf16[128,2560]{1,0:T(8,128)(2,1)} %refs_1_.3), custom_call_target="tpu_custom_call" | custom-call | tf_op jit(solution)/shard_map/pack_pair/pallas_call | solution.py:193
  47.4 22.9 %all_to_all.50.refs_0_ = bf16[4,2,128,640]{3,2,1,0:T(8,128)(2,1)} all-to-all(bf16[4,2,128,640]{3,2,1,0:T(8,128)(2,1)} %pack_pair.1), channel_id=1, replica_groups=mesh['z'=4,'p'=4,'tp'=2] {'p'}, dimensions={0} | all-to-all | bytes 2621440 | tf_op jit(solution)/shard_map/all_to_all | solution.py:235
  70.3 40.9 %place_pair.1 = bf16[2,4,128,640]{3,2,1,0:T(8,128)(2,1)} custom-call(bf16[4,2,128,640]{3,2,1,0:T(8,128)(2,1)} %all_to_all.50.refs_0_), custom_call_target="tpu_custom_call" | custom-call | tf_op jit(solution)/shard_map/place_pair/pallas_call | solution.py:193
  112.2 3.3 %all-to-all-start.2 = ((f32[4,8,128]{2,1,0:T(8,128)}), f32[4,8,128]{2,1,0:T(8,128)S(1)}, u32[]{:S(2)}, u32[]{:S(2)}) async-start(f32[4,8,128]{2,1,0:T(8,128)} %maximum_bitcast_fusion), calls=%async_computation.2 | async-start | bytes 32768 | tf_op jit(solution)/shard_map/all_to_all | solution.py:235
  115.4 17.1 %pack_tokens.1 = bf16[4,128,512]{2,1,0:T(8,128)(2,1)} custom-call(bf16[128,512]{1,0:T(8,128)(2,1)} %refs_0_.2, bf16[128,512]{1,0:T(8,128)(2,1)} %refs_1_.2, bf16[128,512]{1,0:T(8,128)(2,1)} %refs_2_.1, bf16[128,512]{1,0:T(8,128)(2,1)} %refs_3_.1), custom_call_target="tpu_custom_call" | custom-call | tf_op jit(solution)/shard_map/pack_tokens/pallas_call | solution.py:193
  132.6 4.2 %all-to-all-start.1 = ((bf16[4,128,512]{2,1,0:T(8,128)(2,1)}), bf16[4,128,512]{2,1,0:T(8,128)(2,1)S(1)}, u32[]{:S(2)}, u32[]{:S(2)}) async-start(bf16[4,128,512]{2,1,0:T(8,128)(2,1)} %pack_tokens.1), calls=%async_computation.1 | async-start | bytes 1048576 | tf_op jit(solution)/shard_map/all_to_all | solution.py:235
  136.7 6.9 %all-to-all-done.1 = bf16[4,128,512]{2,1,0:T(8,128)(2,1)S(1)} async-done(((bf16[4,128,512]{2,1,0:T(8,128)(2,1)}), bf16[4,128,512]{2,1,0:T(8,128)(2,1)S(1)}, u32[]{:S(2)}, u32[]{:S(2)}) %all-to-all-start.1) | async-done | bytes 524320 | tf_op jit(solution)/shard_map/all_to_all | solution.py:235
  143.6 3.5 %all-to-all-start.7 = ((bf16[4,640,128]{2,1,0:T(8,128)(2,1)}), bf16[4,640,128]{2,1,0:T(8,128)(2,1)S(1)}, u32[]{:S(2)}, u32[]{:S(2)}) async-start(bf16[4,640,128]{2,1,0:T(8,128)(2,1)} %bitcast.52), calls=%async_computation.7 | async-start | bytes 1310720 | tf_op jit(solution)/shard_map/all_to_all | solution.py:235
  147.1 23.5 %delta_rule.1 = (f32[2,512,128]{2,1,0:T(8,128)}, f32[512,128]{1,0:T(8,128)}, f32[2,128,256]{2,1,0:T(8,128)}) custom-call(bf16[512,512]{1,0:T(8,128)(2,1)} %bitcast.45, f32[8,512]{1,0:T(8,128)} %bitcast.53), custom_call_target="tpu_custom_call" | custom-call | tf_op jit(solution)/shard_map/delta_rule/pallas_call | solution.py:153
  172.6 4.8 %all-to-all-start.3 = ((f32[4,128,256]{2,1,0:T(8,128)}), f32[4,128,256]{2,1,0:T(8,128)S(1)}, u32[]{:S(2)}, u32[]{:S(2)}) async-start(f32[4,128,256]{2,1,0:T(8,128)} %broadcast_select_fusion), calls=%async_computation.3 | async-start | bytes 1048576 | tf_op jit(solution)/shard_map/all_to_all | solution.py:235
  177.3 21.0 %place_narrow.1 = bf16[640,512]{1,0:T(8,128)(2,1)} custom-call(bf16[4,640,128]{2,1,0:T(8,128)(2,1)} %copy-done.2), custom_call_target="tpu_custom_call" | custom-call | tf_op jit(solution)/shard_map/place_narrow/pallas_call | solution.py:193
  198.4 8.9 %all-to-all-done.3.maps_ref = f32[4,128,256]{2,1,0:T(8,128)S(1)} async-done(((f32[4,128,256]{2,1,0:T(8,128)}), f32[4,128,256]{2,1,0:T(8,128)S(1)}, u32[]{:S(2)}, u32[]{:S(2)}) %all-to-all-start.3) | async-done | bytes 524320 | tf_op jit(solution)/shard_map/all_to_all | solution.py:235
  208.5 4.3 %all-to-all-start = ((bf16[4,128,1024]{2,1,0:T(8,128)(2,1)}), bf16[4,128,1024]{2,1,0:T(8,128)(2,1)}, u32[]{:S(2)}, u32[]{:S(2)}) async-start(bf16[4,128,1024]{2,1,0:T(8,128)(2,1)} %broadcast_in_dim.50), calls=%async_computation | async-start | bytes 2097152 | tf_op jit(solution)/shard_map/all_to_all | solution.py:235
  212.8 1.6 slice.52.valve_ref
  214.4 3.0 finish.1
  217.4 11.8 %all-gather = bf16[2048,128]{1,0:T(8,128)(2,1)S(1)} all-gather(bf16[512,128]{1,0:T(8,128)(2,1)} %finish.1), channel_id=2, replica_groups=mesh['z'=4,'p'=4,'tp'=2] {'p'}, dimensions={0}, use_global_device_ids=true | all-gather | bytes 655360 | tf_op jit(solution)/shard_map/all_gather | solution.py:328
  229.5 4.6 %all_to_all.51 = bf16[2,512,512]{1,2,0:T(8,128)(2,1)S(1)} all-to-all(bf16[2,512,512]{1,2,0:T(8,128)(2,1)S(1)} %broadcast_in_dim.57), channel_id=1, replica_groups=mesh['z'=4,'p'=4,'tp'=2] {'tp'}, dimensions={0} | all-to-all | bytes 2097152 | tf_op jit(solution)/shard_map/all_to_all | solution.py:235
  234.1 3.5 %fusion.5 = bf16[512,1024]{1,0:T(8,128)(2,1)} fusion(bf16[512,1024]{1,0:T(8,128)(2,1)} %bitcast.22, bf16[512,1024]{0,1:T(8,128)(2,1)S(1)} %bitcast.51, bf16[1024,1024]{1,0:T(8,128)(2,1)S(1)} %copy-done), kind=kOutput, calls=%fused_computation.10 | convolution fusion | flops 1075314688 | bytes 5242880 | tf_op jit(solution)/shard_map/dot_general | solution.py:330
  237.6 1.5 copy.26
  239.3 5.4 %all_to_all.52 = bf16[2,512,1024]{1,2,0:T(8,128)(2,1)S(1)} all-to-all(bf16[2,512,1024]{1,2,0:T(8,128)(2,1)S(1)} %broadcast_in_dim.58), channel_id=1, replica_groups=mesh['z'=4,'p'=4,'tp'=2] {'tp'}, dimensions={0} | all-to-all | bytes 4194304 | tf_op jit(solution)/shard_map/all_to_all | solution.py:235
  245.2 1.9 fusion.2
  247.1 4.2 %fusion.8 = bf16[512,640]{1,0:T(8,128)(2,1)S(1)} fusion(bf16[512,2048]{0,1:T(8,128)(2,1)} %bitcast.49, bf16[2,2048,640]{2,1,0:T(8,128)(2,1)} %all-gather.4.cloned.1.call-done), kind=kOutput, calls=%fused_computation.14 | convolution fusion | flops 1342504960 | bytes 5373952 | tf_op jit(solution)/shard_map/dot_general | solution.py:338
  252.7 1.3 collective-permute-start.1
  254.9 3.4 %collective-permute-done.1 = bf16[1,640]{1,0:T(2,128)(2,1)S(1)} collective-permute-done((bf16[1,640]{1,0:T(2,128)(2,1)S(1)}, bf16[1,640]{1,0:T(2,128)(2,1)S(1)}, u32[]{:S(2)}, u32[]{:S(2)}) %collective-permute-start.1) | collective-permute-done | bytes 1312 | tf_op jit(solution)/shard_map/ppermute | solution.py:341
  258.5 5.5 %fusion.7.hidden_ref = bf16[512,640]{1,0:T(8,128)(2,1)} fusion(bf16[512,2048]{0,1:T(8,128)(2,1)} %bitcast.50, bf16[2,2048,640]{2,1,0:T(8,128)(2,1)} %all-gather.4.cloned.1.call-done, f32[514,640]{1,0:T(8,128)S(1)} %maximum_convert_fusion, f32[640]{0:T(1024)S(1)} %get-tuple-element.13, f32[640]{0:T(1024)S(1)} %get-tuple-element.12, ...), kind=kOutput, calls=%fused_computation.13 | convolution fusion | flops 1345781760 | bytes 9313792 | tf_op jit(solution)/shard_map/dot_general | solution.py:339
  264.0 11.1 %all-gather.6.cloned.1.call-done.weight_ref = bf16[640,2048]{1,0:T(8,128)(2,1)} async-done(((bf16[640,512]{1,0:T(8,128)(2,1)}), bf16[640,2048]{1,0:T(8,128)(2,1)}) %all-gather.6.cloned.1.call-update) | async-done | bytes 2621456 | tf_op jit(solution)/shard_map/all_gather | solution.py:295
  275.1 5.3 %down.1 = bf16[2,512,1024]{2,1,0:T(8,128)(2,1)} custom-call(bf16[512,640]{1,0:T(8,128)(2,1)} %fusion.7.hidden_ref, bf16[640,2048]{1,0:T(8,128)(2,1)} %all-gather.6.cloned.1.call-done.weight_ref), custom_call_target="tpu_custom_call" | custom-call | tf_op jit(solution)/shard_map/down/pallas_call | solution.py:221
  280.4 8.6 %all_to_all.53 = bf16[2,512,1024]{2,1,0:T(8,128)(2,1)} all-to-all(bf16[2,512,1024]{2,1,0:T(8,128)(2,1)} %down.1), channel_id=1, replica_groups=mesh['z'=4,'p'=4,'tp'=2] {'tp'}, dimensions={0} | all-to-all | bytes 4194304 | tf_op jit(solution)/shard_map/all_to_all | solution.py:235
  288.9 3.3 %reduce_sum.31 = bf16[512,1024]{1,0:T(8,128)(2,1)} reduce(bf16[2,512,1024]{2,1,0:T(8,128)(2,1)} %all_to_all.53, bf16[]{:T(256)} %constant.34.clone.1), dimensions={0}, to_apply=%region_1.2 | reduce | flops 524288 | bytes 3145730 | tf_op jit(solution)/shard_map/reduce_sum | solution.py:347
  292.3 3.6 %all-to-all-start.9 = ((bf16[4,128,1024]{2,1,0:T(8,128)(2,1)}), bf16[4,128,1024]{2,1,0:T(8,128)(2,1)S(1)}, u32[]{:S(2)}, u32[]{:S(2)}) async-start(bf16[4,128,1024]{2,1,0:T(8,128)(2,1)} %bitcast.44), calls=%async_computation.9 | async-start | bytes 2097152 | tf_op jit(solution)/shard_map/all_to_all | solution.py:235
  295.9 14.1 %all-to-all-done.9 = bf16[4,128,1024]{2,1,0:T(8,128)(2,1)S(1)} async-done(((bf16[4,128,1024]{2,1,0:T(8,128)(2,1)}), bf16[4,128,1024]{2,1,0:T(8,128)(2,1)S(1)}, u32[]{:S(2)}, u32[]{:S(2)}) %all-to-all-start.9) | async-done | bytes 1048608 | tf_op jit(solution)/shard_map/all_to_all | solution.py:235
  310.2 1.7 add_convert_fusion
  (54 shorter events, 7.6 us)
Async XLA Ops:
  6.5 227.6 %copy-start = (bf16[1024,1024]{1,0:T(8,128)(2,1)S(1)}, bf16[1024,1024]{1,0:T(8,128)(2,1)}, u32[]{:S(2)}) copy-start(bf16[1024,1024]{1,0:T(8,128)(2,1)} %param.26) | copy-start | bytes 6291460
  6.5 240.6 %all-gather.4.cloned.1.call-start = ((), (), s32[]{:S(2)}) async-start(), calls=%async_computation.10 | async-start | bytes 6553600 | tf_op jit(solution)/shard_map/all_gather | solution.py:287
  70.3 40.9 %copy-start.10 = (f32[2,4]{1,0:T(2,128)S(1)}, f32[2,4]{1,0:T(2,128)}, u32[]{:S(2)}) copy-start(f32[2,4]{1,0:T(2,128)} %param.22) | copy-start | bytes 100
  70.3 40.9 %copy-start.7 = (f32[2,4,128]{2,1,0:T(4,128)S(1)}, f32[2,4,128]{2,1,0:T(4,128)}, u32[]{:S(2)}) copy-start(f32[2,4,128]{2,1,0:T(4,128)} %param.24) | copy-start | bytes 12292
  70.3 41.0 %copy-start.8 = (f32[2,4,128]{2,1,0:T(4,128)S(1)}, f32[2,4,128]{2,1,0:T(4,128)}, u32[]{:S(2)}) copy-start(f32[2,4,128]{2,1,0:T(4,128)} %param.21) | copy-start | bytes 12292
  70.3 41.0 %copy-start.9 = (f32[2,4,128]{2,1,0:T(4,128)S(1)}, f32[2,4,128]{2,1,0:T(4,128)}, u32[]{:S(2)}) copy-start(f32[2,4,128]{2,1,0:T(4,128)} %param.23) | copy-start | bytes 12292
  112.2 20.4 %all-to-all-start.2 = ((f32[4,8,128]{2,1,0:T(8,128)}), f32[4,8,128]{2,1,0:T(8,128)S(1)}, u32[]{:S(2)}, u32[]{:S(2)}) async-start(f32[4,8,128]{2,1,0:T(8,128)} %maximum_bitcast_fusion), calls=%async_computation.2 | async-start | bytes 32768 | tf_op jit(solution)/shard_map/all_to_all | solution.py:235
  132.6 14.5 %copy-start.5 = (f32[4,8,128]{2,1,0:T(8,128)}, f32[4,8,128]{2,1,0:T(8,128)S(1)}, u32[]{:S(2)}) copy-start(f32[4,8,128]{2,1,0:T(8,128)S(1)} %all-to-all-done.2) | copy-start | bytes 49156
  132.6 11.0 %all-to-all-start.1 = ((bf16[4,128,512]{2,1,0:T(8,128)(2,1)}), bf16[4,128,512]{2,1,0:T(8,128)(2,1)S(1)}, u32[]{:S(2)}, u32[]{:S(2)}) async-start(bf16[4,128,512]{2,1,0:T(8,128)(2,1)} %pack_tokens.1), calls=%async_computation.1 | async-start | bytes 1048576 | tf_op jit(solution)/shard_map/all_to_all | solution.py:235
  143.6 3.5 %copy-start.1 = (bf16[4,128,512]{2,1,0:T(8,128)(2,1)}, bf16[4,128,512]{2,1,0:T(8,128)(2,1)S(1)}, u32[]{:S(2)}) copy-start(bf16[4,128,512]{2,1,0:T(8,128)(2,1)S(1)} %all-to-all-done.1) | copy-start | bytes 1572868
  143.6 29.0 %all-to-all-start.7 = ((bf16[4,640,128]{2,1,0:T(8,128)(2,1)}), bf16[4,640,128]{2,1,0:T(8,128)(2,1)S(1)}, u32[]{:S(2)}, u32[]{:S(2)}) async-start(bf16[4,640,128]{2,1,0:T(8,128)(2,1)} %bitcast.52), calls=%async_computation.7 | async-start | bytes 1310720 | tf_op jit(solution)/shard_map/all_to_all | solution.py:235
  170.6 36.7 %copy-start.4 = (bf16[128,1024]{1,0:T(8,128)(2,1)S(1)}, bf16[128,1024]{1,0:T(8,128)(2,1)}, u32[]{:S(2)}) copy-start(bf16[128,1024]{1,0:T(8,128)(2,1)} %param.16) | copy-start | bytes 786436
  172.6 4.8 %copy-start.2 = (bf16[4,640,128]{2,1,0:T(8,128)(2,1)}, bf16[4,640,128]{2,1,0:T(8,128)(2,1)S(1)}, u32[]{:S(2)}) copy-start(bf16[4,640,128]{2,1,0:T(8,128)(2,1)S(1)} %all-to-all-done.7.refs_0_) | copy-start | bytes 1966084
  172.6 34.7 %all-to-all-start.3 = ((f32[4,128,256]{2,1,0:T(8,128)}), f32[4,128,256]{2,1,0:T(8,128)S(1)}, u32[]{:S(2)}, u32[]{:S(2)}) async-start(f32[4,128,256]{2,1,0:T(8,128)} %broadcast_select_fusion), calls=%async_computation.3 | async-start | bytes 1048576 | tf_op jit(solution)/shard_map/all_to_all | solution.py:235
  177.3 97.8 %all-gather.6.cloned.1.call-start = ((), (), s32[]{:S(2)}) async-start(), calls=%async_computation.11 | async-start | bytes 3276800 | tf_op jit(solution)/shard_map/all_gather | solution.py:295
  198.3 14.5 %copy-start.6 = (f32[2048]{0:T(1024)S(1)}, f32[2048]{0:T(1024)}, u32[]{:S(2)}) copy-start(f32[2048]{0:T(1024)} %param.27) | copy-start | bytes 24580
  207.3 7.1 %copy-start.3 = (f32[4,128,256]{2,1,0:T(8,128)}, f32[4,128,256]{2,1,0:T(8,128)S(1)}, u32[]{:S(2)}) copy-start(f32[4,128,256]{2,1,0:T(8,128)S(1)} %all-to-all-done.3.maps_ref) | copy-start | bytes 1572868
  208.5 20.9 %all-to-all-start = ((bf16[4,128,1024]{2,1,0:T(8,128)(2,1)}), bf16[4,128,1024]{2,1,0:T(8,128)(2,1)}, u32[]{:S(2)}, u32[]{:S(2)}) async-start(bf16[4,128,1024]{2,1,0:T(8,128)(2,1)} %broadcast_in_dim.50), calls=%async_computation | async-start | bytes 2097152 | tf_op jit(solution)/shard_map/all_to_all | solution.py:235
  251.4 3.5 %collective-permute-start = (bf16[1,640]{1,0:T(2,128)(2,1)S(1)}, bf16[1,640]{1,0:T(2,128)(2,1)S(1)}, u32[]{:S(2)}, u32[]{:S(2)}) collective-permute-start(bf16[1,640]{1,0:T(2,128)(2,1)S(1)} %get-tuple-element.14), channel_id=1, source_target_pairs={{0,8},{8,16},{16,24},{1,9},{9,17},{17,25},{2,10},{10,18},{18,26},{... | collective-permute-start | bytes 3848 | tf_op jit(solution)/shard_map/ppermute | solution.py:340
  252.7 5.7 %collective-permute-start.1 = (bf16[1,640]{1,0:T(2,128)(2,1)S(1)}, bf16[1,640]{1,0:T(2,128)(2,1)S(1)}, u32[]{:S(2)}, u32[]{:S(2)}) collective-permute-start(bf16[1,640]{1,0:T(2,128)(2,1)S(1)} %get-tuple-element.15), channel_id=1, source_target_pairs={{8,0},{16,8},{24,16},{9,1},{17,9},{25,17},{10,2},{18,10},{26,18},{... | collective-permute-start | bytes 3848 | tf_op jit(solution)/shard_map/ppermute | solution.py:341
  292.3 17.7 %all-to-all-start.9 = ((bf16[4,128,1024]{2,1,0:T(8,128)(2,1)}), bf16[4,128,1024]{2,1,0:T(8,128)(2,1)S(1)}, u32[]{:S(2)}, u32[]{:S(2)}) async-start(bf16[4,128,1024]{2,1,0:T(8,128)(2,1)} %bitcast.44), calls=%async_computation.9 | async-start | bytes 2097152 | tf_op jit(solution)/shard_map/all_to_all | solution.py:235
Sparse Core Ops, SparseCore 0:
  111.4 109.0 all-gather.3
  222.0 53.0 all-gather.5

commit v3 on v2

--- a/solution.py
+++ b/solution.py
@@ -174,18 +174,9 @@
 
 
 def copy_kernel(*refs, moves, sources):
-    inputs, output, semaphores = refs[:sources], refs[sources], refs[sources + 1]
-    copies = []
-    for index, (source, take, put) in enumerate(moves):
-        copies.append(
-            pltpu.make_async_copy(
-                inputs[source].at[take], output.at[put], semaphores.at[index]
-            )
-        )
-    for copy in copies:
-        copy.start()
-    for copy in copies:
-        copy.wait()
+    output = refs[sources]
+    for source, take, put in moves:
+        output[put] = refs[source][take]
 
 
 def rearrange(arrays, shape, moves, name):
@@ -193,9 +184,8 @@
     return pl.pallas_call(
         functools.partial(copy_kernel, moves=tuple(moves), sources=count),
         out_shape=jax.ShapeDtypeStruct(shape, arrays[0].dtype),
-        in_specs=[pl.BlockSpec(memory_space=pl.ANY)] * count,
-        out_specs=pl.BlockSpec(memory_space=pl.ANY),
-        scratch_shapes=[pltpu.SemaphoreType.DMA((len(moves),))],
+        in_specs=vmem(count),
+        out_specs=pl.BlockSpec(memory_space=pltpu.VMEM),
         name=name,
     )(*arrays)
 

time: 320 us -> 243 us (0.76)
  Pallas kernels: 152 us -> 41 us
  waiting for transfers between devices: 44.4 us -> 78.7 us
    pallas_call x4, Pallas kernels: 120 us -> 9.22 us  [rearrange(): pl.pallas_call(functools.partial(copy_kernel, moves=tuple(moves), sources...]
    all_to_all x6, waiting for transfers between devices: 29.9 us -> 50.5 us  [exchange(): return lax.all_to_all(slots, axis, split_axis=0, concat_axis=0, tiled=True)]
    all_gather x1, waiting for transfers between devices: 11.1 us -> 24.8 us  [body(): narrow_full = lax.all_gather(narrow, 'z', axis=1, tiled=True)]
  transfers between devices with their start and end apart: 10 -> 10, of which waited for: 5 -> 6; matrix products, arithmetic and copies ran while one was open for 8% -> 10% of each run, Pallas kernels for 20% -> 13%
where the time goes in v3:
time: 243 us; the launch traced here: 242 us
  waiting for transfers between devices  78.7 us (32%)
  blocking collectives  53.4 us (22%)
  Pallas kernels  41 us (17%)
  starting transfers between devices  25.8 us (11%)
  between operations  13.6 us (6%)
  matrix products  13.2 us (5%)
  other arithmetic  9.5 us (4%)
  local copies, waits for them, and re-layouts  6.82 us (3%)
    all_to_all x6, waiting for transfers between devices, exchange(): return lax.all_to_all(slots, axis, split_axis=0, concat_axis=0, tiled=True)  50.5 us
    all_to_all x4, blocking collectives, exchange(): return lax.all_to_all(slots, axis, split_axis=0, concat_axis=0, tiled=True)  41.5 us
    all_gather x1, waiting for transfers between devices, body(): narrow_full = lax.all_gather(narrow, 'z', axis=1, tiled=True)  24.8 us
    pallas_call x1, Pallas kernels, delta_rule(): pl.pallas_call(functools.partial(delta_kernel, width=width), out_shape=(j...  23.5 us
    all_to_all x6, starting transfers between devices, exchange(): return lax.all_to_all(slots, axis, split_axis=0, concat_axis=0, tiled=True)  23.2 us
    all_gather x1, blocking collectives, body(): heads = to_columns(lax.all_gather(mixed, 'p', axis=0))  12 us
    pallas_call x4, Pallas kernels, rearrange(): pl.pallas_call(functools.partial(copy_kernel, moves=tuple(moves), sources...  9.22 us
    dot_general x1, matrix products, body(): up = jnp.dot(normed, pair[1], preferred_element_type=F32)  5.47 us
  transfers between devices with their start and end apart: 10, of which 6 were waited for; matrix products, arithmetic and copies ran while one was open for 10% of the time, Pallas kernels for 13%

profile of v3, /device:TPU:0, one launch (start us, length us, event | category | flops | bytes accessed | tf_op | source)
XLA Modules:
  0.0 242.1 jit_solution(15033784703242452025)
XLA Ops:
  6.5 2.6 %pack_pair.1 = bf16[4,2,128,640]{3,2,1,0:T(8,128)(2,1)} custom-call(bf16[128,2560]{1,0:T(8,128)(2,1)} %refs_0_.3, bf16[128,2560]{1,0:T(8,128)(2,1)} %refs_1_.3), custom_call_target="tpu_custom_call" | custom-call | tf_op jit(solution)/shard_map/pack_pair/pallas_call | solution.py:184
  9.2 22.9 %all_to_all.50.refs_0_ = bf16[4,2,128,640]{3,2,1,0:T(8,128)(2,1)} all-to-all(bf16[4,2,128,640]{3,2,1,0:T(8,128)(2,1)} %pack_pair.1), channel_id=1, replica_groups=mesh['z'=4,'p'=4,'tp'=2] {'p'}, dimensions={0} | all-to-all | bytes 2621440 | tf_op jit(solution)/shard_map/all_to_all | solution.py:225
  32.1 2.6 %place_pair.1 = bf16[2,4,128,640]{3,2,1,0:T(8,128)(2,1)} custom-call(bf16[4,2,128,640]{3,2,1,0:T(8,128)(2,1)} %all_to_all.50.refs_0_), custom_call_target="tpu_custom_call" | custom-call | tf_op jit(solution)/shard_map/place_pair/pallas_call | solution.py:184
  35.6 3.3 %all-to-all-start.2 = ((f32[4,8,128]{2,1,0:T(8,128)}), f32[4,8,128]{2,1,0:T(8,128)S(1)}, u32[]{:S(2)}, u32[]{:S(2)}) async-start(f32[4,8,128]{2,1,0:T(8,128)} %maximum_bitcast_fusion), calls=%async_computation.2 | async-start | bytes 32768 | tf_op jit(solution)/shard_map/all_to_all | solution.py:225
  38.8 2.0 pack_tokens.1
  40.8 2.7 %all-to-all-done.2 = f32[4,8,128]{2,1,0:T(8,128)S(1)} async-done(((f32[4,8,128]{2,1,0:T(8,128)}), f32[4,8,128]{2,1,0:T(8,128)S(1)}, u32[]{:S(2)}, u32[]{:S(2)}) %all-to-all-start.2) | async-done | bytes 16416 | tf_op jit(solution)/shard_map/all_to_all | solution.py:225
  43.5 3.5 %all-to-all-start.1 = ((bf16[4,128,512]{2,1,0:T(8,128)(2,1)}), bf16[4,128,512]{2,1,0:T(8,128)(2,1)S(1)}, u32[]{:S(2)}, u32[]{:S(2)}) async-start(bf16[4,128,512]{2,1,0:T(8,128)(2,1)} %pack_tokens.1), calls=%async_computation.1 | async-start | bytes 1048576 | tf_op jit(solution)/shard_map/all_to_all | solution.py:225
  47.0 6.5 %all-to-all-done.1 = bf16[4,128,512]{2,1,0:T(8,128)(2,1)S(1)} async-done(((bf16[4,128,512]{2,1,0:T(8,128)(2,1)}), bf16[4,128,512]{2,1,0:T(8,128)(2,1)S(1)}, u32[]{:S(2)}, u32[]{:S(2)}) %all-to-all-start.1) | async-done | bytes 524320 | tf_op jit(solution)/shard_map/all_to_all | solution.py:225
  53.6 3.5 %all-to-all-start.7 = ((bf16[4,640,128]{2,1,0:T(8,128)(2,1)}), bf16[4,640,128]{2,1,0:T(8,128)(2,1)S(1)}, u32[]{:S(2)}, u32[]{:S(2)}) async-start(bf16[4,640,128]{2,1,0:T(8,128)(2,1)} %bitcast.52), calls=%async_computation.7 | async-start | bytes 1310720 | tf_op jit(solution)/shard_map/all_to_all | solution.py:225
  57.1 23.5 %delta_rule.1 = (f32[2,512,128]{2,1,0:T(8,128)}, f32[512,128]{1,0:T(8,128)}, f32[2,128,256]{2,1,0:T(8,128)}) custom-call(bf16[512,512]{1,0:T(8,128)(2,1)} %bitcast.45, f32[8,512]{1,0:T(8,128)} %bitcast.53), custom_call_target="tpu_custom_call" | custom-call | tf_op jit(solution)/shard_map/delta_rule/pallas_call | solution.py:153
  82.5 5.0 %all-to-all-start.3 = ((f32[4,128,256]{2,1,0:T(8,128)}), f32[4,128,256]{2,1,0:T(8,128)S(1)}, u32[]{:S(2)}, u32[]{:S(2)}) async-start(f32[4,128,256]{2,1,0:T(8,128)} %broadcast_select_fusion), calls=%async_computation.3 | async-start | bytes 1048576 | tf_op jit(solution)/shard_map/all_to_all | solution.py:225
  87.6 2.0 place_narrow.1
  89.6 27.2 %all-to-all-done.3.maps_ref = f32[4,128,256]{2,1,0:T(8,128)S(1)} async-done(((f32[4,128,256]{2,1,0:T(8,128)}), f32[4,128,256]{2,1,0:T(8,128)S(1)}, u32[]{:S(2)}, u32[]{:S(2)}) %all-to-all-start.3) | async-done | bytes 524320 | tf_op jit(solution)/shard_map/all_to_all | solution.py:225
  118.1 4.3 %all-to-all-start = ((bf16[4,128,1024]{2,1,0:T(8,128)(2,1)}), bf16[4,128,1024]{2,1,0:T(8,128)(2,1)}, u32[]{:S(2)}, u32[]{:S(2)}) async-start(bf16[4,128,1024]{2,1,0:T(8,128)(2,1)} %broadcast_in_dim.50), calls=%async_computation | async-start | bytes 2097152 | tf_op jit(solution)/shard_map/all_to_all | solution.py:225
  122.4 1.6 slice.52.valve_ref
  124.0 3.0 %finish.1 = bf16[512,128]{1,0:T(8,128)(2,1)} custom-call(s32[1]{0:T(128)} %bitcast.1.place_ref, f32[4,128,256]{2,1,0:T(8,128)} %copy-done.3, f32[2,512,128]{2,1,0:T(8,128)} %get-tuple-element.9.reach_ref, f32[512,128]{1,0:T(8,128)} %get-tuple-element.10.own_ref, bf16[512,128]{1,0:T(8,128)(2,1)} %slice.52.valve_ref, f32[1,128]{1,0:T(1,128)} %bitcast.54), custom_call_target="tpu_custom_call" | custom-call | tf_op jit(solution)/shard_map/finish/pallas_call | solution.py:167
  127.0 12.0 %all-gather = bf16[2048,128]{1,0:T(8,128)(2,1)S(1)} all-gather(bf16[512,128]{1,0:T(8,128)(2,1)} %finish.1), channel_id=2, replica_groups=mesh['z'=4,'p'=4,'tp'=2] {'p'}, dimensions={0}, use_global_device_ids=true | all-gather | bytes 655360 | tf_op jit(solution)/shard_map/all_gather | solution.py:318
  139.3 4.6 %all_to_all.51 = bf16[2,512,512]{1,2,0:T(8,128)(2,1)S(1)} all-to-all(bf16[2,512,512]{1,2,0:T(8,128)(2,1)S(1)} %broadcast_in_dim.57), channel_id=1, replica_groups=mesh['z'=4,'p'=4,'tp'=2] {'tp'}, dimensions={0} | all-to-all | bytes 2097152 | tf_op jit(solution)/shard_map/all_to_all | solution.py:225
  143.8 3.5 %fusion.5 = bf16[512,1024]{1,0:T(8,128)(2,1)} fusion(bf16[512,1024]{1,0:T(8,128)(2,1)} %bitcast.22, bf16[512,1024]{0,1:T(8,128)(2,1)S(1)} %bitcast.51, bf16[1024,1024]{1,0:T(8,128)(2,1)S(1)} %copy-done), kind=kOutput, calls=%fused_computation.10 | convolution fusion | flops 1075314688 | bytes 5242880 | tf_op jit(solution)/shard_map/dot_general | solution.py:320
  147.4 1.5 copy.26
  149.0 5.4 %all_to_all.52 = bf16[2,512,1024]{1,2,0:T(8,128)(2,1)S(1)} all-to-all(bf16[2,512,1024]{1,2,0:T(8,128)(2,1)S(1)} %broadcast_in_dim.58), channel_id=1, replica_groups=mesh['z'=4,'p'=4,'tp'=2] {'tp'}, dimensions={0} | all-to-all | bytes 4194304 | tf_op jit(solution)/shard_map/all_to_all | solution.py:225
  154.9 1.9 fusion.2
  156.9 4.2 %fusion.8 = bf16[512,640]{1,0:T(8,128)(2,1)S(1)} fusion(bf16[512,2048]{0,1:T(8,128)(2,1)} %bitcast.49, bf16[2,2048,640]{2,1,0:T(8,128)(2,1)} %all-gather.4.cloned.1.call-done), kind=kOutput, calls=%fused_computation.14 | convolution fusion | flops 1342504960 | bytes 5373952 | tf_op jit(solution)/shard_map/dot_general | solution.py:328
  164.7 3.4 %collective-permute-done.1 = bf16[1,640]{1,0:T(2,128)(2,1)S(1)} collective-permute-done((bf16[1,640]{1,0:T(2,128)(2,1)S(1)}, bf16[1,640]{1,0:T(2,128)(2,1)S(1)}, u32[]{:S(2)}, u32[]{:S(2)}) %collective-permute-start.1) | collective-permute-done | bytes 1312 | tf_op jit(solution)/shard_map/ppermute | solution.py:331
  168.2 5.5 %fusion.7.hidden_ref = bf16[512,640]{1,0:T(8,128)(2,1)} fusion(bf16[512,2048]{0,1:T(8,128)(2,1)} %bitcast.50, bf16[2,2048,640]{2,1,0:T(8,128)(2,1)} %all-gather.4.cloned.1.call-done, f32[514,640]{1,0:T(8,128)S(1)} %maximum_convert_fusion, f32[640]{0:T(1024)S(1)} %get-tuple-element.13, f32[640]{0:T(1024)S(1)} %get-tuple-element.12, ...), kind=kOutput, calls=%fused_computation.13 | convolution fusion | flops 1345781760 | bytes 9313792 | tf_op jit(solution)/shard_map/dot_general | solution.py:329
  173.7 24.8 %all-gather.6.cloned.1.call-done.weight_ref = bf16[640,2048]{1,0:T(8,128)(2,1)} async-done(((bf16[640,512]{1,0:T(8,128)(2,1)}), bf16[640,2048]{1,0:T(8,128)(2,1)}) %all-gather.6.cloned.1.call-update) | async-done | bytes 2621456 | tf_op jit(solution)/shard_map/all_gather | solution.py:285
  198.5 5.3 %down.1 = bf16[2,512,1024]{2,1,0:T(8,128)(2,1)} custom-call(bf16[512,640]{1,0:T(8,128)(2,1)} %fusion.7.hidden_ref, bf16[640,2048]{1,0:T(8,128)(2,1)} %all-gather.6.cloned.1.call-done.weight_ref), custom_call_target="tpu_custom_call" | custom-call | tf_op jit(solution)/shard_map/down/pallas_call | solution.py:211
  203.7 8.6 %all_to_all.53 = bf16[2,512,1024]{2,1,0:T(8,128)(2,1)} all-to-all(bf16[2,512,1024]{2,1,0:T(8,128)(2,1)} %down.1), channel_id=1, replica_groups=mesh['z'=4,'p'=4,'tp'=2] {'tp'}, dimensions={0} | all-to-all | bytes 4194304 | tf_op jit(solution)/shard_map/all_to_all | solution.py:225
  212.3 3.3 %reduce_sum.31 = bf16[512,1024]{1,0:T(8,128)(2,1)} reduce(bf16[2,512,1024]{2,1,0:T(8,128)(2,1)} %all_to_all.53, bf16[]{:T(256)} %constant.34.clone.1), dimensions={0}, to_apply=%region_1.2 | reduce | flops 524288 | bytes 3145730 | tf_op jit(solution)/shard_map/reduce_sum | solution.py:337
  215.7 3.7 %all-to-all-start.9 = ((bf16[4,128,1024]{2,1,0:T(8,128)(2,1)}), bf16[4,128,1024]{2,1,0:T(8,128)(2,1)S(1)}, u32[]{:S(2)}, u32[]{:S(2)}) async-start(bf16[4,128,1024]{2,1,0:T(8,128)(2,1)} %bitcast.44), calls=%async_computation.9 | async-start | bytes 2097152 | tf_op jit(solution)/shard_map/all_to_all | solution.py:225
  219.3 14.0 %all-to-all-done.9 = bf16[4,128,1024]{2,1,0:T(8,128)(2,1)S(1)} async-done(((bf16[4,128,1024]{2,1,0:T(8,128)(2,1)}), bf16[4,128,1024]{2,1,0:T(8,128)(2,1)S(1)}, u32[]{:S(2)}, u32[]{:S(2)}) %all-to-all-start.9) | async-done | bytes 1048608 | tf_op jit(solution)/shard_map/all_to_all | solution.py:225
  233.5 1.7 add_convert_fusion
  (54 shorter events, 8.9 us)
Async XLA Ops:
  6.5 137.3 %copy-start = (bf16[1024,1024]{1,0:T(8,128)(2,1)S(1)}, bf16[1024,1024]{1,0:T(8,128)(2,1)}, u32[]{:S(2)}) copy-start(bf16[1024,1024]{1,0:T(8,128)(2,1)} %param.26) | copy-start | bytes 6291460
  6.5 150.3 %all-gather.4.cloned.1.call-start = ((), (), s32[]{:S(2)}) async-start(), calls=%async_computation.10 | async-start | bytes 6553600 | tf_op jit(solution)/shard_map/all_gather | solution.py:277
  32.0 2.6 %copy-start.10 = (f32[2,4]{1,0:T(2,128)S(1)}, f32[2,4]{1,0:T(2,128)}, u32[]{:S(2)}) copy-start(f32[2,4]{1,0:T(2,128)} %param.22) | copy-start | bytes 100
  32.0 2.6 %copy-start.7 = (f32[2,4,128]{2,1,0:T(4,128)S(1)}, f32[2,4,128]{2,1,0:T(4,128)}, u32[]{:S(2)}) copy-start(f32[2,4,128]{2,1,0:T(4,128)} %param.24) | copy-start | bytes 12292
  32.0 2.6 %copy-start.8 = (f32[2,4,128]{2,1,0:T(4,128)S(1)}, f32[2,4,128]{2,1,0:T(4,128)}, u32[]{:S(2)}) copy-start(f32[2,4,128]{2,1,0:T(4,128)} %param.21) | copy-start | bytes 12292
  32.0 2.7 %copy-start.9 = (f32[2,4,128]{2,1,0:T(4,128)S(1)}, f32[2,4,128]{2,1,0:T(4,128)}, u32[]{:S(2)}) copy-start(f32[2,4,128]{2,1,0:T(4,128)} %param.23) | copy-start | bytes 12292
  35.6 7.9 %all-to-all-start.2 = ((f32[4,8,128]{2,1,0:T(8,128)}), f32[4,8,128]{2,1,0:T(8,128)S(1)}, u32[]{:S(2)}, u32[]{:S(2)}) async-start(f32[4,8,128]{2,1,0:T(8,128)} %maximum_bitcast_fusion), calls=%async_computation.2 | async-start | bytes 32768 | tf_op jit(solution)/shard_map/all_to_all | solution.py:225
  43.5 13.5 %copy-start.5 = (f32[4,8,128]{2,1,0:T(8,128)}, f32[4,8,128]{2,1,0:T(8,128)S(1)}, u32[]{:S(2)}) copy-start(f32[4,8,128]{2,1,0:T(8,128)S(1)} %all-to-all-done.2) | copy-start | bytes 49156
  43.5 10.0 %all-to-all-start.1 = ((bf16[4,128,512]{2,1,0:T(8,128)(2,1)}), bf16[4,128,512]{2,1,0:T(8,128)(2,1)S(1)}, u32[]{:S(2)}, u32[]{:S(2)}) async-start(bf16[4,128,512]{2,1,0:T(8,128)(2,1)} %pack_tokens.1), calls=%async_computation.1 | async-start | bytes 1048576 | tf_op jit(solution)/shard_map/all_to_all | solution.py:225
  53.6 3.5 %copy-start.1 = (bf16[4,128,512]{2,1,0:T(8,128)(2,1)}, bf16[4,128,512]{2,1,0:T(8,128)(2,1)S(1)}, u32[]{:S(2)}) copy-start(bf16[4,128,512]{2,1,0:T(8,128)(2,1)S(1)} %all-to-all-done.1) | copy-start | bytes 1572868
  53.6 29.0 %all-to-all-start.7 = ((bf16[4,640,128]{2,1,0:T(8,128)(2,1)}), bf16[4,640,128]{2,1,0:T(8,128)(2,1)S(1)}, u32[]{:S(2)}, u32[]{:S(2)}) async-start(bf16[4,640,128]{2,1,0:T(8,128)(2,1)} %bitcast.52), calls=%async_computation.7 | async-start | bytes 1310720 | tf_op jit(solution)/shard_map/all_to_all | solution.py:225
  80.6 36.3 %copy-start.4 = (bf16[128,1024]{1,0:T(8,128)(2,1)S(1)}, bf16[128,1024]{1,0:T(8,128)(2,1)}, u32[]{:S(2)}) copy-start(bf16[128,1024]{1,0:T(8,128)(2,1)} %param.16) | copy-start | bytes 786436
  82.5 5.1 %copy-start.2 = (bf16[4,640,128]{2,1,0:T(8,128)(2,1)}, bf16[4,640,128]{2,1,0:T(8,128)(2,1)S(1)}, u32[]{:S(2)}) copy-start(bf16[4,640,128]{2,1,0:T(8,128)(2,1)S(1)} %all-to-all-done.7.refs_0_) | copy-start | bytes 1966084
  82.5 34.4 %all-to-all-start.3 = ((f32[4,128,256]{2,1,0:T(8,128)}), f32[4,128,256]{2,1,0:T(8,128)S(1)}, u32[]{:S(2)}, u32[]{:S(2)}) async-start(f32[4,128,256]{2,1,0:T(8,128)} %broadcast_select_fusion), calls=%async_computation.3 | async-start | bytes 1048576 | tf_op jit(solution)/shard_map/all_to_all | solution.py:225
  87.6 110.9 %all-gather.6.cloned.1.call-start = ((), (), s32[]{:S(2)}) async-start(), calls=%async_computation.11 | async-start | bytes 3276800 | tf_op jit(solution)/shard_map/all_gather | solution.py:285
  89.6 32.8 %copy-start.6 = (f32[2048]{0:T(1024)S(1)}, f32[2048]{0:T(1024)}, u32[]{:S(2)}) copy-start(f32[2048]{0:T(1024)} %param.27) | copy-start | bytes 24580
  116.9 7.1 %copy-start.3 = (f32[4,128,256]{2,1,0:T(8,128)}, f32[4,128,256]{2,1,0:T(8,128)S(1)}, u32[]{:S(2)}) copy-start(f32[4,128,256]{2,1,0:T(8,128)S(1)} %all-to-all-done.3.maps_ref) | copy-start | bytes 1572868
  118.1 21.1 %all-to-all-start = ((bf16[4,128,1024]{2,1,0:T(8,128)(2,1)}), bf16[4,128,1024]{2,1,0:T(8,128)(2,1)}, u32[]{:S(2)}, u32[]{:S(2)}) async-start(bf16[4,128,1024]{2,1,0:T(8,128)(2,1)} %broadcast_in_dim.50), calls=%async_computation | async-start | bytes 2097152 | tf_op jit(solution)/shard_map/all_to_all | solution.py:225
  161.1 3.5 %collective-permute-start = (bf16[1,640]{1,0:T(2,128)(2,1)S(1)}, bf16[1,640]{1,0:T(2,128)(2,1)S(1)}, u32[]{:S(2)}, u32[]{:S(2)}) collective-permute-start(bf16[1,640]{1,0:T(2,128)(2,1)S(1)} %get-tuple-element.14), channel_id=1, source_target_pairs={{0,8},{8,16},{16,24},{1,9},{9,17},{17,25},{2,10},{10,18},{18,26},{... | collective-permute-start | bytes 3848 | tf_op jit(solution)/shard_map/ppermute | solution.py:330
  162.4 5.7 %collective-permute-start.1 = (bf16[1,640]{1,0:T(2,128)(2,1)S(1)}, bf16[1,640]{1,0:T(2,128)(2,1)S(1)}, u32[]{:S(2)}, u32[]{:S(2)}) collective-permute-start(bf16[1,640]{1,0:T(2,128)(2,1)S(1)} %get-tuple-element.15), channel_id=1, source_target_pairs={{8,0},{16,8},{24,16},{9,1},{17,9},{25,17},{10,2},{18,10},{26,18},{... | collective-permute-start | bytes 3848 | tf_op jit(solution)/shard_map/ppermute | solution.py:331
  215.7 17.7 %all-to-all-start.9 = ((bf16[4,128,1024]{2,1,0:T(8,128)(2,1)}), bf16[4,128,1024]{2,1,0:T(8,128)(2,1)S(1)}, u32[]{:S(2)}, u32[]{:S(2)}) async-start(bf16[4,128,1024]{2,1,0:T(8,128)(2,1)} %bitcast.44), calls=%async_computation.9 | async-start | bytes 2097152 | tf_op jit(solution)/shard_map/all_to_all | solution.py:225
Sparse Core Ops, SparseCore 0:
  34.8 109.0 all-gather.3
  145.4 53.0 all-gather.5
